TPU v7x, 32 devices: a whole 2x2x4 slice. The times are simulated.
32 devices in a mesh: grp: 2 (over y), sp: 8 (over z, core), tp: 2 (over x).
Axes of the slice: x: 2, y: 2, z: 4, core: 2. Of those that a mesh axis runs over, the one named last changes fastest.
Arguments:
- tokens: bfloat16 [12288, 2048], P(('grp', 'sp'), 'tp'), parts along dimension 0, may hold values from -4000 to 4000
- gain: float32 [2048], replicated, may hold values from 0.1 to 1.9
- w_query: bfloat16 [2048, 1024], P('sp', 'tp'), may hold values from -1 to 1
- w_key: bfloat16 [2048, 256], P('sp', 'tp'), may hold values from -1 to 1
- w_value: bfloat16 [2048, 256], P('sp', 'tp'), may hold values from -0.125 to 0.125
- w_input: bfloat16 [2048, 1024], P('sp', 'tp'), may hold values from -0.125 to 0.125
- w_bgate: bfloat16 [2048, 1024], P('sp', 'tp'), may hold values from -0.125 to 0.125
- w_cgate: bfloat16 [2048, 1024], P('sp', 'tp'), may hold values from -0.125 to 0.125
- w_attn_out: bfloat16 [1024, 2048], P('sp', 'tp'), may hold values from -2 to 2
- w_conv_out: bfloat16 [1024, 2048], P('sp', 'tp'), may hold values from -0.1875 to 0.1875
- sink_logit: float32 [16], P('tp'), may hold values from 0 to 5
- taps: float32 [3, 1024], P(None, 'tp'), may hold values from -3.5 to 3.5
- conv_bias: float32 [1024], P('tp'), may hold values from -4 to 4
- documents: int32 [12288], P(('grp', 'sp')), parts along dimension 0, may hold values from 0 to 3, never falling along the last dimension, each value on 1 to 3072 neighbouring positions
Outputs:
- mixed: bfloat16 [12288, 2048], P(('grp', 'sp'), 'tp'), parts along dimension 0
There are 2 independent parts, one for each index of `grp`. A program takes and returns all parts, laid end to end along the dimension named above; an argument that names none is the same for every part. Nothing has to cross between parts.
All inputs are finite; a program needn't handle non-finite values.
Results may differ from a plain program's by a relative error of at most 0.013.
The roundings to bfloat16 on the way count: a program that leaves them out, or rounds other values in their place, can miss the bound.
Values may be sent and summed in bfloat16 or wider, within the bound.
A program may use at most 64 MiB of HBM per device.

v0:
```python
import functools

import jax
import jax.numpy as jnp
from jax import lax
from jax.experimental import pallas as pl
from jax.experimental.pallas import tpu as pltpu
from jax.sharding import PartitionSpec as P

HEAD_DIM = 64
WINDOW = 128


EPS = 1e-06
THETA = 500000.0
CONV_UNITS = 4
ATT_UNITS = 2
OUT_UNITS = 2
LATE = 3
TOKEN_CHUNKS = 4


def fused_plan(grp_count, sp_count, tp_count, rows, part, proj_rows, out_rows, q_width, k_width, c_width):
    lines = sp_count // 2
    return (
        grp_count == 2
        and tp_count == 2
        and sp_count % 2 == 0
        and 2 <= lines <= 4
        and proj_rows % (2 * CONV_UNITS * 16) == 0
        and proj_rows % (2 * ATT_UNITS * 16) == 0
        and out_rows % (2 * OUT_UNITS * 16) == 0
        and rows % (TOKEN_CHUNKS * 16) == 0
        and rows % (2 * WINDOW) == 0
        and part % 256 == 0
        and q_width % 256 == 0
        and k_width == 128
        and c_width % 256 == 0
        and 2 * HEAD_DIM == 128
    )


def layer_kernel(
    sizes,
    tok_ref,
    gain_ref,
    wk_ref,
    wv_ref,
    wc_ref,
    wu_ref,
    wb_ref,
    wq_ref,
    wa_ref,
    wm_ref,
    sink_ref,
    taps_ref,
    bias_ref,
    doc_ref,
    doc_col,
    cos_ref,
    sin_ref,
    out_ref,
    wp_full,
    wo_full,
    tok_other,
    scaled,
    inv_ref,
    proj_ref,
    pair_ext,
    query_s,
    carried,
    carry_near,
    doc_row,
    convolved,
    conv_other,
    attended,
    att_other,
    z_send,
    z_recv,
    y_send,
    y_recv,
    dz_send,
    dz_recv,
    dy_send,
    dy_recv,
    do_send,
    do_recv,
    x_send,
    x_recv,
    own_sem,
    halo_send,
    halo_recv,
    conv_sem,
    att_send,
    att_recv,
):
    lines, rp, ro = sizes
    f32 = jnp.float32
    rows, part = tok_ref.shape
    bf16 = jnp.bfloat16
    k_width, c_width, q_width = wk_ref.shape[1], wc_ref.shape[1], wq_ref.shape[1]
    k_at = 3 * c_width
    q_at = k_at + 2 * k_width
    width = q_at + q_width
    y = lax.axis_index("grp")
    sp = lax.axis_index("sp")
    x = lax.axis_index("tp")
    z, c = sp // 2, sp % 2
    groups_of = []
    for full, size, count, cols in (
        (wp_full, rp, CONV_UNITS, (0, k_at)),
        (wp_full, rp, ATT_UNITS, (k_at, width)),
        (wo_full, ro, OUT_UNITS, (0, 2 * part)),
    ):
        groups_of += [(full, size, size // 2 // count, j, cols) for j in range(count)]
    ends = (CONV_UNITS, CONV_UNITS + ATT_UNITS, CONV_UNITS + ATT_UNITS + OUT_UNITS)
    units_of = (range(0, ends[0]), range(ends[0], ends[1]), range(ends[1], ends[2]))
    to_y = {"grp": 1 - y}
    to_core = {"sp": z * 2 + 1 - c}
    to_x = {"tp": 1 - x}
    to_z = ({"sp": sp + 2}, {"sp": sp - 2})
    has_next = (z < lines - 1, z > 0)

    def origin(way, t):
        return z - t if way == 0 else z + t

    def arrives(way, t):
        return z >= t if way == 0 else z < lines - t

    def place(u, zo, cc, h):
        full, size, tall, j, cols = groups_of[u]
        row = (zo * 2 + cc) * size + h * (size // 2) + j * tall
        return full.at[pl.ds(pl.multiple_of(row, tall), tall), cols[0] : cols[1]]

    def remote(src, dst, send, recv, device):
        return pltpu.make_async_remote_copy(
            src_ref=src, dst_ref=dst, send_sem=send, recv_sem=recv,
            device_id=device, device_id_type=pl.DeviceIdType.MESH,
        )

    def z_copy(way, t, u):
        zo = origin(way, t)
        dst = place(u, zo, c, y)
        return remote(dst, dst, z_send.at[way, t, u], z_recv.at[way, t, u], to_z[way])

    def z_arrival(way, t, u):
        dst = place(u, origin(way, t), c, y)
        return remote(dst, dst, z_send.at[way, t - 1, u], z_recv.at[way, t - 1, u], to_z[way])

    def y_copy(way, t, u):
        ref = place(u, origin(way, t), c, y)
        return remote(ref, ref, y_send.at[way, t - 1, u], y_recv.at[way, t - 1, u], to_y)

    def y_arrival(way, t, u):
        ref = place(u, origin(way, t), c, 1 - y)
        return remote(ref, ref, y_send.at[way, t - 1, u], y_recv.at[way, t - 1, u], to_y)

    def d_copy(kind, way, t, u, cc):
        send, recv = (dz_send, dz_recv) if kind == 0 else (dy_send, dy_recv)
        ref = place(u, origin(way, t), cc, y if kind == 0 else 1 - y)
        return remote(ref, ref, send.at[way, t - 1, u], recv.at[way, t - 1, u], to_core)

    def shard(group, cc):
        full, size, _, _, cols = groups_of[ends[group] - 1]
        return full, pl.ds(pl.multiple_of((z * 2 + cc) * size, size), size), cols

    def own_d(group, cc):
        full, at, cols = shard(group, cc)
        dst = full.at[at, cols[0] : cols[1]]
        return remote(dst, dst, do_send.at[group], do_recv.at[group], to_core)

    own_refs = ((wc_ref, wu_ref, wb_ref), (wk_ref, wv_ref, wq_ref), (wa_ref, wm_ref))

    def own_local(group):
        full, at, cols = shard(group, c)
        copies, col = [], cols[0]
        for j, ref in enumerate(own_refs[group]):
            size = ref.shape[1]
            copies.append(
                pltpu.make_async_copy(
                    ref, full.at[at, col : col + size], own_sem.at[3 * group + j]
                )
            )
            col += size
        return copies

    chunk = rows // TOKEN_CHUNKS

    def x_copy(k):
        return remote(
            tok_ref.at[pl.ds(k * chunk, chunk), :], tok_other.at[pl.ds(k * chunk, chunk), :],
            x_send.at[k], x_recv.at[k], to_x,
        )

    last = 2 * lines - 1
    steps_sp = (sp + 1, sp - 1)
    sends_to = (sp < last, sp > 0)
    gets_from = (sp > 0, sp < last)
    side = jnp.where(c == 0, sp - 1, sp + 1)
    has_side = (side >= 0) & (side <= last)

    def halo(kind, way):
        if kind == 0:
            src = doc_ref.at[:, rows - WINDOW : rows] if way == 0 else doc_ref.at[:, 0:WINDOW]
            at = 0 if way == 0 else WINDOW + rows
            dst = doc_row.at[:, at : at + WINDOW]
        elif kind == 1:
            at = rows if way == 0 else WINDOW
            src = pair_ext.at[at : at + WINDOW, :]
            at = 0 if way == 0 else WINDOW + rows
            dst = pair_ext.at[at : at + WINDOW, :]
        else:
            at = rows - 16 if way == 0 else 0
            src = carried.at[at : at + 16, :]
            dst = carry_near.at[way]
        return remote(
            src, dst, halo_send.at[kind, way], halo_recv.at[kind, way], {"sp": steps_sp[way]}
        )

    def start_halo(kind):
        for way in range(2):

            @pl.when(sends_to[way])
            def _():
                halo(kind, way).start()

    def wait_halo(kind):
        for way in range(2):

            @pl.when(gets_from[way])
            def _():
                halo(kind, way).wait_recv()

    def conv_copy():
        return remote(convolved, conv_other, conv_sem.at[0], conv_sem.at[1], to_x)

    def att_copy(i):
        at = pl.ds(pl.multiple_of(i * WINDOW, WINDOW), WINDOW)
        return remote(attended.at[at, :], att_other.at[at, :], att_send.at[i], att_recv.at[i], to_x)

    for copy in own_local(0) + own_local(1) + own_local(2):
        copy.start()

    barrier = pltpu.get_barrier_semaphore()
    for device in (to_y, to_core, to_x):
        pl.semaphore_signal(barrier, inc=1, device_id=device, device_id_type=pl.DeviceIdType.MESH)
    for way in range(2):

        @pl.when(has_next[way])
        def _():
            pl.semaphore_signal(
                barrier, inc=1, device_id=to_z[way], device_id_type=pl.DeviceIdType.MESH
            )

    @pl.when(has_side)
    def _():
        pl.semaphore_signal(
            barrier, inc=1, device_id={"sp": side}, device_id_type=pl.DeviceIdType.MESH
        )

    neighbours = jnp.where(has_side, 1, 0) + jnp.where(z > 0, 1, 0) + jnp.where(z < lines - 1, 1, 0) + 3
    pl.semaphore_wait(barrier, neighbours)

    def start_own(units):
        for u in units:
            for way in range(2):

                @pl.when(has_next[way])
                def _():
                    z_copy(way, 0, u).start()

    for k in range(TOKEN_CHUNKS):
        x_copy(k).start()
    for copy in own_local(0):
        copy.wait()
    start_own(units_of[0])
    own_d(0, c).start()
    start_halo(0)
    doc_row[:, WINDOW : WINDOW + rows] = doc_ref[...]

    @pl.when(sp == 0)
    def _():
        doc_row[:, :WINDOW] = jnp.full((doc_row.shape[0], WINDOW), -1.0, f32)
        pair_ext[:WINDOW, :] = jnp.zeros((WINDOW, pair_ext.shape[1]), bf16)

    @pl.when(sp == last)
    def _():
        doc_row[:, WINDOW + rows :] = jnp.full((doc_row.shape[0], WINDOW), -1.0, f32)
        pair_ext[WINDOW + rows :, :] = jnp.zeros((WINDOW, pair_ext.shape[1]), bf16)


    def event(t, u):
        for way in range(2):

            @pl.when(arrives(way, t))
            def _():
                z_arrival(way, t, u).wait_recv()
                if t < lines - 1:

                    @pl.when(has_next[way])
                    def _():
                        z_copy(way, t, u).start()

                y_copy(way, t, u).start()
                d_copy(0, way, t, u, c).start()

    def y_event(t, u):
        for way in range(2):

            @pl.when(arrives(way, t))
            def _():
                y_arrival(way, t, u).wait_recv()
                d_copy(1, way, t, u, c).start()

    def scale(k):
        x_copy(k).wait_recv()
        tile = 32

        def body(i, carry):
            at = pl.ds(pl.multiple_of(k * chunk + i * tile, tile), tile)
            own = tok_ref[at, :].astype(f32)
            other = tok_other[at, :].astype(f32)
            total = jnp.sum(own * own, axis=1, keepdims=True) + jnp.sum(
                other * other, axis=1, keepdims=True
            )
            inv_ref[at, :] = jnp.broadcast_to(
                lax.rsqrt(total / (2 * part) + EPS), (tile, inv_ref.shape[1])
            )
            mine_at = pl.multiple_of(x * part, part)
            other_at = pl.multiple_of((1 - x) * part, part)
            scaled[at, pl.ds(mine_at, part)] = (own * gain_ref[:, pl.ds(mine_at, part)]).astype(
                scaled.dtype
            )
            scaled[at, pl.ds(other_at, part)] = (
                other * gain_ref[:, pl.ds(other_at, part)]
            ).astype(scaled.dtype)
            return carry

        lax.fori_loop(0, chunk // tile, body, 0)

    queue, marks = [], []
    for units in units_of:
        queue += [(t, u) for t in range(1, lines) for u in units]
        marks.append(len(queue))
    openers = {marks[g] - len(units_of[g]): g + 1 for g in range(2)}
    state = [0, 0]

    def advance(goal):
        while state[0] < goal:
            i = state[0]
            event(*queue[i])
            if i in openers:
                group = openers[i]
                for copy in own_local(group):
                    copy.wait()
                start_own(units_of[group])
                own_d(group, c).start()
            state[0] += 1
            while state[1] < state[0] - LATE:
                y_event(*queue[state[1]])
                state[1] += 1

    def settle(group):
        advance(marks[group])
        while state[1] < marks[group]:
            y_event(*queue[state[1]])
            state[1] += 1
        own_d(group, 1 - c).wait_recv()
        for t, u in queue[marks[group - 1] if group else 0 : marks[group]]:
            for way in range(2):

                @pl.when(arrives(way, t))
                def _():
                    d_copy(0, way, t, u, 1 - c).wait_recv()
                    d_copy(1, way, t, u, 1 - c).wait_recv()

    for k in range(TOKEN_CHUNKS - 1):
        advance(marks[0] * (k + 1) // (TOKEN_CHUNKS - 1))
        scale(k)
    advance(marks[0] + 2)
    settle(0)
    scale(TOKEN_CHUNKS - 1)

    cut = 256
    c_at, u_at, b_at = 0, c_width, 2 * c_width

    def project(begin, end):
        def body(j, carry):
            at = pl.ds(pl.multiple_of(j * cut, cut), cut)
            acc = jnp.dot(scaled[...], wp_full[:, at], preferred_element_type=f32)
            proj_ref[:, at] = acc * inv_ref[:, :1]
            return carry

        lax.fori_loop(begin // cut, end // cut, body, 0)

    lanes = 128
    lane = lax.broadcasted_iota(jnp.int32, (rows, lanes), 1)
    low = (lane % HEAD_DIM) < HEAD_DIM // 2

    def turned(cells):
        ahead = pltpu.roll(cells, lanes - HEAD_DIM // 2, 1)
        behind = pltpu.roll(cells, HEAD_DIM // 2, 1)
        return cells * cos_ref[...] + jnp.where(low, ahead, behind) * sin_ref[...]

    def block(at, j):
        return pl.ds(pl.multiple_of(at + j * lanes, lanes), lanes)

    project(c_at, b_at)

    def carry_body(j, carry):
        carried[:, block(0, j)] = (
            proj_ref[:, block(c_at, j)] * proj_ref[:, block(u_at, j)]
        ).astype(bf16)
        return carry

    lax.fori_loop(0, c_width // lanes, carry_body, 0)
    advance(marks[0] + 3)
    start_halo(2)
    project(b_at, k_at)
    advance(marks[0] + 4)
    wait_halo(0)
    wait_halo(2)

    row = lax.broadcasted_iota(jnp.int32, (rows, lanes), 0)

    def conv_body(j, carry):
        at = block(0, j)
        docs = doc_col[...]
        cells = carried[:, at].astype(f32)
        before = jnp.where(row == 0, carry_near[0, 15:16, at].astype(f32), pltpu.roll(cells, 1, 0))
        after = jnp.where(
            row == rows - 1, carry_near[1, 0:1, at].astype(f32), pltpu.roll(cells, rows - 1, 0)
        )
        doc_before = jnp.where(row == 0, doc_row[0:1, WINDOW - 1 : WINDOW], pltpu.roll(docs, 1, 0))
        doc_after = jnp.where(
            row == rows - 1,
            doc_row[0:1, WINDOW + rows : WINDOW + rows + 1],
            pltpu.roll(docs, rows - 1, 0),
        )
        conv = jnp.where(doc_before == docs, before * taps_ref[0:1, at], 0.0)
        conv = conv + cells * taps_ref[1:2, at]
        conv = conv + jnp.where(doc_after == docs, after * taps_ref[2:3, at], 0.0)
        convolved[:, at] = (proj_ref[:, block(b_at, j)] * (conv + bias_ref[:, at])).astype(bf16)
        return carry

    lax.fori_loop(0, c_width // lanes, conv_body, 0)
    conv_copy().start()
    settle(1)
    project(k_at, q_at)
    keys_at = slice(k_at, k_at + k_width)
    pair_ext[WINDOW : WINDOW + rows, :k_width] = turned(proj_ref[:, keys_at]).astype(bf16)
    pair_ext[WINDOW : WINDOW + rows, k_width:] = proj_ref[:, k_at + k_width : q_at].astype(bf16)
    start_halo(1)
    advance(marks[1] + 1)
    project(q_at, width)
    advance(marks[1] + 2)

    def query_body(j, carry):
        cells = turned(proj_ref[:, block(q_at, j)])
        query_s[:, block(0, j)] = (cells * HEAD_DIM ** (-0.5)).astype(bf16)
        return carry

    lax.fori_loop(0, q_width // lanes, query_body, 0)
    wait_halo(1)
    kv_heads = k_width // HEAD_DIM
    groups = q_width // HEAD_DIM // kv_heads
    span = 3 * WINDOW
    gap = lax.broadcasted_iota(jnp.int32, (WINDOW, span), 1) - lax.broadcasted_iota(
        jnp.int32, (WINDOW, span), 0
    )
    window = (gap >= 0) & (gap <= 2 * WINDOW)

    def attend(i, carry):
        at = pl.ds(pl.multiple_of(i * WINDOW, WINDOW), WINDOW)
        near = pl.ds(pl.multiple_of(i * WINDOW, WINDOW), span)
        allowed = window & (doc_col[at, 0:1] == doc_row[0:1, near])
        bias = jnp.where(allowed, 0.0, -jnp.inf)
        bias = jnp.concatenate([bias] * groups, axis=0)
        queries = query_s[at, :]
        pairs = pair_ext[near, :]
        for head in range(kv_heads):
            keys = pairs[:, head * HEAD_DIM : (head + 1) * HEAD_DIM]
            values = pairs[:, k_width + head * HEAD_DIM : k_width + (head + 1) * HEAD_DIM]
            first = head * groups
            stack = jnp.concatenate(
                [
                    queries[:, (first + g) * HEAD_DIM : (first + g + 1) * HEAD_DIM]
                    for g in range(groups)
                ],
                axis=0,
            )
            sinks = jnp.concatenate(
                [jnp.full((WINDOW, 1), sink_ref[first + g], f32) for g in range(groups)], axis=0
            )
            scores = lax.dot_general(
                stack, keys, (((1,), (1,)), ((), ())), preferred_element_type=f32
            )
            scores = scores + bias
            top = jnp.maximum(jnp.max(scores, axis=1, keepdims=True), sinks)
            expo = jnp.exp(scores - top)
            total = jnp.sum(expo, axis=1, keepdims=True) + jnp.exp(sinks - top)
            weight = (expo * (1.0 / total)).astype(bf16)
            result = jnp.dot(weight, values, preferred_element_type=f32).astype(bf16)
            wide = jnp.concatenate(
                [result[g * WINDOW : (g + 1) * WINDOW] for g in range(groups)], axis=1
            )
            attended[at, first * HEAD_DIM : (first + groups) * HEAD_DIM] = wide

        @pl.when(i > 0)
        def _():
            att_copy(i - 1).start()

        return carry

    blocks = rows // WINDOW
    lax.fori_loop(0, blocks // 2, attend, 0)
    advance(marks[1] + 4)
    lax.fori_loop(blocks // 2, blocks, attend, 0)
    att_copy(blocks - 1).start()
    settle(2)
    conv_copy().wait_recv()
    q_mine = pl.ds(pl.multiple_of(x * q_width, q_width), q_width)
    q_yours = pl.ds(pl.multiple_of((1 - x) * q_width, q_width), q_width)
    c_mine = pl.ds(pl.multiple_of(x * c_width, c_width), c_width)
    c_yours = pl.ds(pl.multiple_of((1 - x) * c_width, c_width), c_width)

    def mix_body(j, carry):
        at = pl.ds(pl.multiple_of(j * cut, cut), cut)
        late = pl.ds(pl.multiple_of(part + j * cut, cut), cut)
        acc = jnp.dot(attended[...], wo_full[q_mine, at], preferred_element_type=f32)
        acc = acc + jnp.dot(convolved[...], wo_full[c_mine, late], preferred_element_type=f32)
        acc = acc + jnp.dot(conv_other[...], wo_full[c_yours, late], preferred_element_type=f32)
        proj_ref[:, at] = acc
        return carry

    lax.fori_loop(0, part // cut, mix_body, 0)
    half = rows // 2
    for k in range(2):
        for i in range(k * blocks // 2, (k + 1) * blocks // 2):
            att_copy(i).wait_recv()

        def last_body(j, carry):
            at = pl.ds(pl.multiple_of(j * cut, cut), cut)
            acc = proj_ref[k * half : (k + 1) * half, at] + jnp.dot(
                att_other[k * half : (k + 1) * half, :],
                wo_full[q_yours, at],
                preferred_element_type=f32,
            )
            out_ref[k * half : (k + 1) * half, at] = acc.astype(bf16)
            return carry

        lax.fori_loop(0, part // cut, last_body, 0)

    for kind in range(3):
        for way in range(2):

            @pl.when(sends_to[way])
            def _():
                halo(kind, way).wait_send()

    conv_copy().wait_send()
    for i in range(blocks):
        att_copy(i).wait_send()
    for group in range(3):
        own_d(group, c).wait_send()
    for k in range(TOKEN_CHUNKS):
        x_copy(k).wait_send()
    for u in range(ends[2]):
        for way in range(2):

            @pl.when(has_next[way])
            def _():
                z_copy(way, 0, u).wait_send()

            for t in range(1, lines):

                @pl.when(arrives(way, t))
                def _():
                    if t < lines - 1:

                        @pl.when(has_next[way])
                        def _():
                            z_copy(way, t, u).wait_send()

                    y_copy(way, t, u).wait_send()
                    d_copy(0, way, t, u, c).wait_send()
                    d_copy(1, way, t, u, c).wait_send()


def fused_layer(
    tokens, gain, projections, outputs, sink_logit, taps, conv_bias, documents, sp_count
):
    rows, part = tokens.shape
    f32 = jnp.float32
    bf16 = jnp.bfloat16
    lines = sp_count // 2
    wk, wv, wc, wu, wb, wq = projections
    width = sum(w.shape[1] for w in projections)
    rp, ro = wq.shape[0], outputs[0].shape[0]
    q_width, k_width, c_width = wq.shape[1], wk.shape[1], wc.shape[1]
    half = HEAD_DIM // 2
    lanes = 128
    positions = lax.axis_index("sp") * rows + jnp.arange(rows, dtype=jnp.int32)
    freq = jnp.power(THETA, -(jnp.arange(half, dtype=f32) * (2.0 / HEAD_DIM)))
    angle = positions.astype(f32)[:, None] * freq[None, :]
    cosine, sine = jnp.cos(angle), jnp.sin(angle)
    cosine = jnp.concatenate([cosine] * (lanes // half), axis=1)
    sine = jnp.concatenate([-sine, sine] * (lanes // HEAD_DIM), axis=1)
    docs = documents.astype(f32)
    doc_rows = jnp.broadcast_to(docs[None, :], (8, rows))
    doc_cols = jnp.broadcast_to(docs[:, None], (rows, lanes))
    blocks = rows // WINDOW
    dma = pltpu.SemaphoreType.DMA
    hops = (2, lines - 1, CONV_UNITS + ATT_UNITS + OUT_UNITS)
    vmem = pl.BlockSpec(memory_space=pltpu.VMEM)
    hbm = pl.BlockSpec(memory_space=pl.ANY)
    smem = pl.BlockSpec(memory_space=pltpu.SMEM)
    flops = 2 * rows * 2 * part * width
    return pl.pallas_call(
        functools.partial(layer_kernel, (lines, rp, ro)),
        out_shape=jax.ShapeDtypeStruct((rows, part), bf16),
        in_specs=[vmem] * 2 + [hbm] * 8 + [smem] + [vmem] * 6,
        out_specs=vmem,
        scratch_shapes=[
            pltpu.VMEM((rp * sp_count, width), bf16),
            pltpu.VMEM((ro * sp_count, 2 * part), bf16),
            pltpu.VMEM((rows, part), bf16),
            pltpu.VMEM((rows, 2 * part), bf16),
            pltpu.VMEM((rows, 128), f32),
            pltpu.VMEM((rows, max(width, part)), f32),
            pltpu.VMEM((rows + 2 * WINDOW, 2 * k_width), bf16),
            pltpu.VMEM((rows, q_width), bf16),
            pltpu.VMEM((rows, c_width), bf16),
            pltpu.VMEM((2, 16, c_width), bf16),
            pltpu.VMEM((8, rows + 2 * WINDOW), f32),
            pltpu.VMEM((rows, c_width), bf16),
            pltpu.VMEM((rows, c_width), bf16),
            pltpu.VMEM((rows, q_width), bf16),
            pltpu.VMEM((rows, q_width), bf16),
        ]
        + [dma(hops)] * 8
        + [dma((3,)), dma((3,)), dma((TOKEN_CHUNKS,)), dma((TOKEN_CHUNKS,)), dma((9,))]
        + [dma((3, 2)), dma((3, 2)), dma((2,)), dma((blocks,)), dma((blocks,))],
        compiler_params=pltpu.CompilerParams(
            collective_id=0, has_side_effects=True, vmem_limit_bytes=62 * 1024 * 1024
        ),
        cost_estimate=pl.CostEstimate(flops=flops, bytes_accessed=0, transcendentals=0),
        name="layer",
    )(
        tokens,
        gain[None, :],
        *projections,
        *outputs,
        sink_logit,
        taps,
        conv_bias[None, :],
        doc_rows,
        doc_cols,
        cosine,
        sine,
    )


def extended(cells, sides, width):
    for axis, dim in sides:
        count = lax.axis_size(axis)
        ends = count - 1
        head = lax.slice_in_dim(cells, 0, width, axis=dim)
        tail = lax.slice_in_dim(cells, cells.shape[dim] - width, cells.shape[dim], axis=dim)
        cells = jnp.concatenate(
            [
                lax.ppermute(tail, axis, [(i, (i + 1) % count) for i in range(ends)]),
                cells,
                lax.ppermute(head, axis, [((i + 1) % count, i) for i in range(ends)]),
            ],
            axis=dim,
        )
    return cells


def rotate(proj, positions, heads):
    rows = proj.shape[0]
    size = proj.shape[1] // heads
    half = size // 2
    freq = jnp.power(THETA, -(jnp.arange(half, dtype=jnp.float32) * (2.0 / size)))
    angle = positions.astype(jnp.float32)[:, None] * freq[None, :]
    cosine = jnp.cos(angle)[:, None, :]
    sine = jnp.sin(angle)[:, None, :]
    shaped = proj.reshape(rows, heads, size)
    first = shaped[..., :half]
    second = shaped[..., half:]
    turned = jnp.concatenate(
        [first * cosine - second * sine, second * cosine + first * sine], axis=-1
    )
    return turned.reshape(rows, heads * size)


def sink_softmax(scores, allowed, sinks):
    masked = jnp.where(allowed, scores, -jnp.inf)
    top = jnp.maximum(jnp.max(masked, axis=-1, keepdims=True), sinks)
    expo = jnp.exp(masked - top)
    return expo / (jnp.sum(expo, axis=-1, keepdims=True) + jnp.exp(sinks - top))


def local(
    tokens,
    gain,
    w_query,
    w_key,
    w_value,
    w_input,
    w_bgate,
    w_cgate,
    w_attn_out,
    w_conv_out,
    sink_logit,
    taps,
    conv_bias,
    documents,
):
    f32 = jnp.float32
    bf16 = jnp.bfloat16
    rows, part = tokens.shape
    tp_count = lax.axis_size("tp")
    sp_count = lax.axis_size("sp")
    width = part * tp_count
    head_dim = HEAD_DIM
    q_local = w_query.shape[1] // head_dim
    kv_local = w_key.shape[1] // head_dim
    groups = q_local // kv_local
    if fused_plan(
        lax.axis_size("grp"),
        sp_count,
        tp_count,
        rows,
        part,
        w_query.shape[0],
        w_attn_out.shape[0],
        w_query.shape[1],
        w_key.shape[1],
        w_input.shape[1],
    ):
        return fused_layer(
            tokens,
            gain,
            (w_key, w_value, w_cgate, w_input, w_bgate, w_query),
            (w_attn_out, w_conv_out),
            sink_logit,
            taps,
            conv_bias,
            documents,
            sp_count,
        )
    wq, wk, wv, wu, wb, wc, w_attn, w_conv = (
        lax.all_gather(w_query, "sp", axis=0, tiled=True),
        lax.all_gather(w_key, "sp", axis=0, tiled=True),
        lax.all_gather(w_value, "sp", axis=0, tiled=True),
        lax.all_gather(w_input, "sp", axis=0, tiled=True),
        lax.all_gather(w_bgate, "sp", axis=0, tiled=True),
        lax.all_gather(w_cgate, "sp", axis=0, tiled=True),
        lax.all_gather(w_attn_out, "sp", axis=0, tiled=True),
        lax.all_gather(w_conv_out, "sp", axis=0, tiled=True),
    )
    matrices = (wq, wk, wv, wu, wb, wc)
    piece_f = lax.all_gather(tokens, "tp", axis=1, tiled=True).astype(f32)
    scaled = (piece_f * gain[None, :]).astype(bf16)
    products = tuple((jnp.dot(scaled, mat, preferred_element_type=f32) for mat in matrices))
    folded = products + (jnp.sum(piece_f * piece_f, axis=1),)
    sums = folded[:6]
    squares = folded[6]
    inv = lax.rsqrt(squares / width + EPS)[:, None]
    q_acc, k_acc, v_acc, u_acc, b_acc, c_acc = sums
    positions = lax.axis_index("sp") * rows + jnp.arange(rows, dtype=jnp.int32)
    query = rotate(q_acc * inv, positions, q_local).astype(bf16)
    keys = rotate(k_acc * inv, positions, kv_local).astype(bf16)
    values = (v_acc * inv).astype(bf16)
    carried = (c_acc * inv * (u_acc * inv)).astype(bf16)
    bgate = b_acc * inv
    doc_col = documents.astype(f32).astype(bf16)[:, None]
    paired = jnp.concatenate([keys, values], axis=1)
    pair_ext, doc_ext = (
        extended(paired, (("sp", 0),), WINDOW),
        extended(doc_col, (("sp", 0),), WINDOW),
    )
    carry_ext, doc_near = (extended(carried, (("sp", 0),), 1), extended(doc_col, (("sp", 0),), 1))
    key_width = kv_local * head_dim
    key_ext = pair_ext[:, :key_width].reshape(-1, kv_local, head_dim)
    val_ext = pair_ext[:, key_width:].reshape(-1, kv_local, head_dim)
    key_doc = doc_ext[:, 0].astype(f32)
    own_doc = doc_col[:, 0].astype(f32)
    key_pos = positions[0] - WINDOW + jnp.arange(rows + 2 * WINDOW, dtype=jnp.int32)
    total = sp_count * rows
    sinks = sink_logit.reshape(kv_local, groups, 1, 1)
    block = rows // 2
    outputs = []
    for begin in range(0, rows, block):
        span = block + 2 * WINDOW
        q_block = query[begin : begin + block].reshape(block, kv_local, groups, head_dim)
        k_block = key_ext[begin : begin + span]
        v_block = val_ext[begin : begin + span]
        q_pos = positions[begin : begin + block]
        k_pos = key_pos[begin : begin + span]
        scores = jnp.einsum(
            "qhgd,khd->hgqk", q_block, k_block, preferred_element_type=f32
        ) * head_dim ** (-0.5)
        allowed = jnp.abs(q_pos[:, None] - k_pos[None, :]) <= WINDOW
        allowed = allowed & (
            own_doc[begin : begin + block, None] == key_doc[None, begin : begin + span]
        )
        allowed = allowed & (k_pos >= 0)[None, :] & (k_pos < total)[None, :]
        weight = sink_softmax(scores, allowed, sinks).astype(bf16)
        result = jnp.einsum("hgqk,khd->qhgd", weight, v_block, preferred_element_type=f32)
        outputs.append(result.astype(bf16).reshape(block, q_local * head_dim))
    attended = jnp.concatenate(outputs, axis=0)
    near_doc = doc_near[:, 0].astype(f32)
    conv = jnp.zeros((rows, carried.shape[1]), f32)
    for tap in range(3):
        same = (near_doc[tap : tap + rows] == near_doc[1 : rows + 1])[:, None]
        conv = conv + jnp.where(
            same, carry_ext[tap : tap + rows].astype(f32) * taps[tap][None, :], 0.0
        )
    convolved = (bgate * (conv + conv_bias[None, :])).astype(bf16)
    acc = jnp.dot(
        lax.all_gather(attended, "tp", axis=1, tiled=True), w_attn, preferred_element_type=f32
    )
    mixed = acc + jnp.dot(
        lax.all_gather(convolved, "tp", axis=1, tiled=True), w_conv, preferred_element_type=f32
    )
    return mixed.astype(bf16)


def solution(mesh):
    placed = (
        P(("grp", "sp"), "tp"),
        P(),
        P("sp", "tp"),
        P("sp", "tp"),
        P("sp", "tp"),
        P("sp", "tp"),
        P("sp", "tp"),
        P("sp", "tp"),
        P("sp", "tp"),
        P("sp", "tp"),
        P("tp"),
        P(None, "tp"),
        P("tp"),
        P(("grp", "sp")),
    )
    return jax.shard_map(
        local, mesh=mesh, in_specs=placed, out_specs=P(("grp", "sp"), "tp"), check_vma=False
    )
```

profile of v0, /device:TPU:0, one launch (start us, length us, event | category | flops | bytes accessed | tf_op | source)
XLA Modules:
  0.0 107.9 jit_solution(13014142136066516883)
XLA Ops:
  0.0 0.7 convert_element_type.10
  0.7 0.6 broadcast_in_dim.10.doc_ref
  1.3 0.9 broadcast_in_dim.11.doc_col
  2.2 1.4 %fusion = (f32[768,32]{1,0:T(8,128)S(1)}, f32[768,32]{1,0:T(8,128)S(1)}, f32[768,32]{1,0:T(8,128)S(1)}) fusion(f32[32]{0:T(128)S(1)} %negate_power_fusion, f32[768]{0:T(1024)S(1)} %add_convert_fusion), kind=kLoop, calls=%fused_computation.4 | loop fusion | flops 49152 | bytes 298112 | tf_op jit(solution)/shard_map/neg | solution.py:608
  3.7 1.6 %pad_maximum_fusion = (f32[768,128]{1,0:T(8,128)}, f32[768,128]{1,0:T(8,128)}) fusion(f32[768,32]{1,0:T(8,128)S(1)} %get-tuple-element.7, f32[768,32]{1,0:T(8,128)S(1)} %get-tuple-element.6, f32[768,32]{1,0:T(8,128)S(1)} %get-tuple-element.5), kind=kLoop, calls=%fused_computation.2 | loop fusion | flops 589824 | bytes 1081344 | tf_op jit(solution)/shard_map/concatenate | solution.py:607
  5.3 100.0 %layer.1 = bf16[768,1024]{1,0:T(8,128)(2,1)} custom-call(bf16[768,1024]{1,0:T(8,128)(2,1)} %tok_ref.1, f32[1,2048]{1,0:T(1,128)} %bitcast.2, bf16[256,128]{1,0:T(8,128)(2,1)} %wk_ref.1, bf16[256,128]{1,0:T(8,128)(2,1)} %wv_ref.1, bf16[256,512]{1,0:T(8,128)(2,1)} %wc_ref.1, bf16[256,512]{1,0:T(8,128)(2,1)} %wu_ref.1, bf16[256,512]{1,0:T(8,128)(2,1)} %wb_ref.1, ...), custom_call_target="tpu_custom_call" | custom-call | flops 7247757312 | tf_op jit(solution)/shard_map/layer/pallas_call | solution.py:619
  105.3 2.7 %copy.17 = bf16[768,1024]{1,0:T(8,128)(2,1)} copy(bf16[768,1024]{1,0:T(8,128)(2,1)} %layer.1) | data formatting | bytes 3145728
  (2 shorter events, 0.0 us)
where the time goes:
time: 109 us; the launch traced here: 108 us
  Pallas kernels  100 us (92%)
  local copies, waits for them, and re-layouts  4.18 us (4%)
  other arithmetic  3.73 us (3%)
    pallas_call x1, Pallas kernels, fused_layer(): pl.pallas_call(functools.partial(layer_kernel, (lines, rp, ro)), out_shap...  100 us
    unnamed x1, local copies, waits for them, and re-layouts  2.67 us

commit v1 on v0

v1 whole, which is shorter than its diff:
```python
import functools

import jax
import jax.numpy as jnp
import numpy as np
from jax import lax
from jax.experimental import pallas as pl
from jax.experimental.pallas import tpu as pltpu
from jax.sharding import PartitionSpec as P

HEAD_DIM = 64
WINDOW = 128


EPS = 1e-06
THETA = 500000.0
ATT_UNITS = 2
CONV_UNITS = 4
OUT_UNITS = 2
LATE = 3
CHUNK = 256
LANES = 128


def fused_plan(grp_count, sp_count, tp_count, rows, part, proj_rows, out_rows, q_width, k_width, c_width):
    lines = sp_count // 2
    return (
        grp_count == 2
        and tp_count == 2
        and sp_count % 2 == 0
        and lines == 4
        and proj_rows % (2 * CONV_UNITS * 16) == 0
        and proj_rows % (2 * ATT_UNITS * 16) == 0
        and out_rows % (2 * OUT_UNITS * 16) == 0
        and rows % CHUNK == 0
        and 3 * CHUNK <= rows <= 1024
        and CHUNK == 2 * WINDOW
        and WINDOW == LANES
        and part % 256 == 0
        and q_width % 256 == 0
        and k_width == LANES
        and c_width % 256 == 0
        and 2 * HEAD_DIM == LANES
    )


def layer_kernel(
    sizes,
    tok_hbm,
    gain_ref,
    wk_ref,
    wv_ref,
    wc_ref,
    wu_ref,
    wb_ref,
    wq_ref,
    wa_ref,
    wm_ref,
    sink_ref,
    taps_ref,
    bias_ref,
    doc_ref,
    freq_ref,
    out_ref,
    wp_full,
    wo_full,
    tok_own,
    tok_other,
    scaled,
    inv_ref,
    proj_ref,
    acc_ref,
    stage,
    pair_ext,
    query_s,
    carried,
    doc_row,
    doc_col,
    turn_ref,
    cos_ref,
    sin_ref,
    convolved,
    conv_other,
    attended,
    att_other,
    z_send,
    z_recv,
    y_send,
    y_recv,
    dz_send,
    dz_recv,
    dy_send,
    dy_recv,
    do_send,
    do_recv,
    x_send,
    x_recv,
    own_sem,
    tok_sem,
    out_sem,
    halo_send,
    halo_recv,
    conv_send,
    conv_recv,
    att_send,
    att_recv,
):
    lines, rp, ro = sizes
    f32 = jnp.float32
    bf16 = jnp.bfloat16
    rows, part = tok_own.shape
    k_width, c_width, q_width = wk_ref.shape[1], wc_ref.shape[1], wq_ref.shape[1]
    k_at = 3 * c_width
    q_at = k_at + 2 * k_width
    width = q_at + q_width
    chunks = rows // CHUNK
    blocks = rows // WINDOW
    order = (chunks - 1,) + tuple(range(chunks - 1))
    y = lax.axis_index("grp")
    sp = lax.axis_index("sp")
    x = lax.axis_index("tp")
    z, c = sp // 2, sp % 2
    counts = (ATT_UNITS, CONV_UNITS, OUT_UNITS)
    fulls = (wp_full, wp_full, wo_full)
    heights = (rp, rp, ro)
    spans = ((k_at, width), (0, k_at), (0, 2 * part))
    first_unit = (0, ATT_UNITS, ATT_UNITS + CONV_UNITS)
    marks = [0]
    for count in counts:
        marks.append(marks[-1] + (lines - 1) * count)
    to_y = {"grp": 1 - y}
    to_core = {"sp": z * 2 + 1 - c}
    to_x = {"tp": 1 - x}
    to_z = ({"sp": sp + 2}, {"sp": sp - 2})
    has_next = (z < lines - 1, z > 0)

    def origin(way, t):
        return z - t if way == 0 else z + t

    def arrives(way, t):
        return z >= t if way == 0 else z < lines - t

    def place(g, j, zo, cc, h):
        size = heights[g]
        tall = size // 2 // counts[g]
        row = (zo * 2 + cc) * size + h * (size // 2) + j * tall
        return fulls[g].at[pl.ds(pl.multiple_of(row, tall), tall), spans[g][0] : spans[g][1]]

    def remote(src, dst, send, recv, device):
        return pltpu.make_async_remote_copy(
            src_ref=src, dst_ref=dst, send_sem=send, recv_sem=recv,
            device_id=device, device_id_type=pl.DeviceIdType.MESH,
        )

    def z_copy(way, t, g, j):
        ref, u = place(g, j, origin(way, t), c, y), first_unit[g] + j
        return remote(ref, ref, z_send.at[way, t, u], z_recv.at[way, t, u], to_z[way])

    def z_arrival(way, t, g, j):
        ref, u = place(g, j, origin(way, t), c, y), first_unit[g] + j
        return remote(ref, ref, z_send.at[way, t - 1, u], z_recv.at[way, t - 1, u], to_z[way])

    def y_copy(way, t, g, j):
        ref, u = place(g, j, origin(way, t), c, y), first_unit[g] + j
        return remote(ref, ref, y_send.at[way, t - 1, u], y_recv.at[way, t - 1, u], to_y)

    def y_arrival(way, t, g, j):
        ref, u = place(g, j, origin(way, t), c, 1 - y), first_unit[g] + j
        return remote(ref, ref, y_send.at[way, t - 1, u], y_recv.at[way, t - 1, u], to_y)

    def d_copy(kind, way, t, g, j, cc):
        send, recv = (dz_send, dz_recv) if kind == 0 else (dy_send, dy_recv)
        ref, u = place(g, j, origin(way, t), cc, y if kind == 0 else 1 - y), first_unit[g] + j
        return remote(ref, ref, send.at[way, t - 1, u], recv.at[way, t - 1, u], to_core)

    def own_rows(g, cc):
        size = heights[g]
        return pl.ds(pl.multiple_of((z * 2 + cc) * size, size), size)

    def own_d(g, cc):
        dst = fulls[g].at[own_rows(g, cc), spans[g][0] : spans[g][1]]
        return remote(dst, dst, do_send.at[g], do_recv.at[g], to_core)

    own_refs = ((wk_ref, wv_ref, wq_ref), (wc_ref, wu_ref, wb_ref), (wa_ref, wm_ref))

    def own_local(g):
        at, copies, col = own_rows(g, c), [], spans[g][0]
        for j, ref in enumerate(own_refs[g]):
            size = ref.shape[1]
            copies.append(
                pltpu.make_async_copy(
                    ref, fulls[g].at[at, col : col + size], own_sem.at[3 * g + j]
                )
            )
            col += size
        return copies

    def tok_local(k):
        at = slice(k * CHUNK, (k + 1) * CHUNK)
        return pltpu.make_async_copy(tok_hbm.at[at, :], tok_own.at[at, :], tok_sem.at[k])

    def x_copy(k):
        at = slice(k * CHUNK, (k + 1) * CHUNK)
        return remote(tok_own.at[at, :], tok_other.at[at, :], x_send.at[k], x_recv.at[k], to_x)

    last = 2 * lines - 1
    steps_sp = (sp + 1, sp - 1)
    sends_to = (sp < last, sp > 0)
    gets_from = (sp > 0, sp < last)
    side = jnp.where(c == 0, sp - 1, sp + 1)
    has_side = (side >= 0) & (side <= last)
    edge = 16

    def halo(kind, way):
        if kind == 0:
            at = rows if way == 0 else WINDOW
            src = doc_row.at[:, at : at + WINDOW]
            at = 0 if way == 0 else WINDOW + rows
            dst = doc_row.at[:, at : at + WINDOW]
        elif kind == 1:
            at = rows if way == 0 else WINDOW
            src = pair_ext.at[at : at + WINDOW, :]
            at = 0 if way == 0 else WINDOW + rows
            dst = pair_ext.at[at : at + WINDOW, :]
        else:
            at = rows if way == 0 else edge
            src = carried.at[at : at + edge, :]
            at = 0 if way == 0 else edge + rows
            dst = carried.at[at : at + edge, :]
        return remote(
            src, dst, halo_send.at[kind, way], halo_recv.at[kind, way], {"sp": steps_sp[way]}
        )

    def start_halo(kind, way):
        @pl.when(sends_to[way])
        def _():
            halo(kind, way).start()

    def wait_halo(kind):
        for way in range(2):

            @pl.when(gets_from[way])
            def _():
                halo(kind, way).wait_recv()

    def conv_copy(k):
        at = slice(k * CHUNK, (k + 1) * CHUNK)
        return remote(
            convolved.at[at, :], conv_other.at[at, :], conv_send.at[k], conv_recv.at[k], to_x
        )

    def att_copy(i):
        at = pl.ds(pl.multiple_of(i * WINDOW, WINDOW), WINDOW)
        return remote(attended.at[at, :], att_other.at[at, :], att_send.at[i], att_recv.at[i], to_x)

    def start_own(g):
        for copy in own_local(g):
            copy.wait()
        for j in range(counts[g]):
            for way in range(2):

                @pl.when(has_next[way])
                def _():
                    z_copy(way, 0, g, j).start()

        own_d(g, c).start()

    def z_event(g, m):
        t, j = m // counts[g] + 1, m % counts[g]
        for way in range(2):

            @pl.when(arrives(way, t))
            def _():
                z_arrival(way, t, g, j).wait_recv()

                @pl.when(has_next[way] & (t < lines - 1))
                def _():
                    z_copy(way, t, g, j).start()

                y_copy(way, t, g, j).start()
                d_copy(0, way, t, g, j, c).start()

    def y_event(g, m):
        t, j = m // counts[g] + 1, m % counts[g]
        for way in range(2):

            @pl.when(arrives(way, t))
            def _():
                y_arrival(way, t, g, j).wait_recv()
                d_copy(1, way, t, g, j, c).start()

    def on(n, act):
        if isinstance(n, int):
            g = max(i for i in range(3) if marks[i] <= n)
            act(g, n - marks[g])
            return
        for g in range(3):

            @pl.when((n >= marks[g]) & (n < marks[g + 1]))
            def _():
                act(g, n - marks[g])

    state = [0, 0]

    def advance(goal):
        while state[0] < goal:
            on(state[0], z_event)
            state[0] += 1
            while state[1] < state[0] - LATE:
                on(state[1], y_event)
                state[1] += 1

    def settle(g):
        advance(marks[g + 1])
        while state[1] < marks[g + 1]:
            on(state[1], y_event)
            state[1] += 1
        own_d(g, 1 - c).wait_recv()

        def arrived(m, carry):
            t, j = m // counts[g] + 1, m % counts[g]
            for way in range(2):

                @pl.when(arrives(way, t))
                def _():
                    d_copy(0, way, t, g, j, 1 - c).wait_recv()
                    d_copy(1, way, t, g, j, 1 - c).wait_recv()

            return carry

        lax.fori_loop(0, marks[g + 1] - marks[g], arrived, 0)

    for k in order:
        tok_local(k).start()
    for g in range(3):
        for copy in own_local(g):
            copy.start()

    barrier = pltpu.get_barrier_semaphore()
    for device in (to_y, to_core, to_x):
        pl.semaphore_signal(barrier, inc=1, device_id=device, device_id_type=pl.DeviceIdType.MESH)
    for way in range(2):

        @pl.when(has_next[way])
        def _():
            pl.semaphore_signal(
                barrier, inc=1, device_id=to_z[way], device_id_type=pl.DeviceIdType.MESH
            )

    @pl.when(has_side)
    def _():
        pl.semaphore_signal(
            barrier, inc=1, device_id={"sp": side}, device_id_type=pl.DeviceIdType.MESH
        )

    docs = doc_ref[...].astype(f32)
    doc_row[:, WINDOW : WINDOW + rows] = jnp.broadcast_to(docs, (doc_row.shape[0], rows))

    @pl.when(sp == 0)
    def _():
        doc_row[:, :WINDOW] = jnp.full((doc_row.shape[0], WINDOW), -1.0, f32)
        pair_ext[:WINDOW, :] = jnp.zeros((WINDOW, pair_ext.shape[1]), bf16)

    @pl.when(sp == last)
    def _():
        doc_row[:, WINDOW + rows :] = jnp.full((doc_row.shape[0], WINDOW), -1.0, f32)
        pair_ext[WINDOW + rows :, :] = jnp.zeros((WINDOW, pair_ext.shape[1]), bf16)

    neighbours = jnp.where(has_side, 1, 0) + jnp.where(z > 0, 1, 0) + jnp.where(z < lines - 1, 1, 0) + 3
    with jax.named_scope("barrier"):
        pl.semaphore_wait(barrier, neighbours)

    for k in order:
        tok_local(k).wait()
        x_copy(k).start()
    start_own(0)
    for way in range(2):
        start_halo(0, way)

    for i in range(blocks):
        at = slice(i * WINDOW, (i + 1) * WINDOW)
        doc_col[at, :] = jnp.broadcast_to(docs[:, at], (WINDOW, LANES)).T

    tile = 32
    lane = lax.broadcasted_iota(jnp.int32, (tile, LANES), 1)
    step = lax.broadcasted_iota(jnp.int32, (tile, LANES), 0)
    freq = freq_ref[...]
    far = (sp * rows + step * tile).astype(f32) * freq
    near_angle = step.astype(f32) * freq
    turn_ref[0:tile, :] = jnp.cos(far)
    turn_ref[tile : 2 * tile, :] = jnp.sin(far)
    near_cos, near_sin = jnp.cos(near_angle), jnp.sin(near_angle)
    sign = jnp.where((lane % HEAD_DIM) < HEAD_DIM // 2, -1.0, 1.0)

    def table_body(i, carry):
        at = pl.ds(pl.multiple_of(i * tile, tile), tile)
        far_cos, far_sin = turn_ref[pl.ds(i, 1), :], turn_ref[pl.ds(tile + i, 1), :]
        cos_ref[at, :] = far_cos * near_cos - far_sin * near_sin
        sin_ref[at, :] = sign * (far_sin * near_cos + far_cos * near_sin)
        return carry

    lax.fori_loop(0, rows // tile, table_body, 0)

    mine_at = pl.multiple_of(x * part, part)
    yours_at = pl.multiple_of((1 - x) * part, part)

    def scale(k):
        x_copy(k).wait_recv()

        def body(i, carry):
            at = pl.ds(pl.multiple_of(k * CHUNK + i * tile, tile), tile)
            own = tok_own[at, :].astype(f32)
            other = tok_other[at, :].astype(f32)
            total = jnp.sum(own * own, axis=1, keepdims=True) + jnp.sum(
                other * other, axis=1, keepdims=True
            )
            inv_ref[at, :] = jnp.broadcast_to(
                lax.rsqrt(total / (2 * part) + EPS), (tile, inv_ref.shape[1])
            )
            scaled[at, pl.ds(mine_at, part)] = (own * gain_ref[:, pl.ds(mine_at, part)]).astype(bf16)
            scaled[at, pl.ds(yours_at, part)] = (
                other * gain_ref[:, pl.ds(yours_at, part)]
            ).astype(bf16)
            return carry

        lax.fori_loop(0, CHUNK // tile, body, 0)

    cut = 256

    def project(k, begin, end):
        mine = slice(k * CHUNK, (k + 1) * CHUNK)

        def body(j, carry):
            at = pl.ds(pl.multiple_of(j * cut, cut), cut)
            acc = jnp.dot(scaled[mine, :], wp_full[:, at], preferred_element_type=f32)
            proj_ref[mine, at] = acc * inv_ref[mine, :1]
            return carry

        lax.fori_loop(begin // cut, end // cut, body, 0)

    lane_c = lax.broadcasted_iota(jnp.int32, (CHUNK, LANES), 1)
    low = (lane_c % HEAD_DIM) < HEAD_DIM // 2

    def block(at, j):
        return pl.ds(pl.multiple_of(at + j * LANES, LANES), LANES)

    def project_att(k):
        mine = slice(k * CHUNK, (k + 1) * CHUNK)
        ext = slice(WINDOW + k * CHUNK, WINDOW + (k + 1) * CHUNK)
        project(k, k_at, width)

        def turned(cells):
            ahead = pltpu.roll(cells, LANES - HEAD_DIM // 2, 1)
            behind = pltpu.roll(cells, HEAD_DIM // 2, 1)
            return cells * cos_ref[mine, :] + jnp.where(low, ahead, behind) * sin_ref[mine, :]

        pair_ext[ext, :k_width] = turned(proj_ref[mine, k_at : k_at + k_width]).astype(bf16)
        pair_ext[ext, k_width:] = proj_ref[mine, k_at + k_width : q_at].astype(bf16)

        def query_body(j, carry):
            cells = turned(proj_ref[mine, block(q_at, j)])
            query_s[mine, block(0, j)] = (cells * HEAD_DIM ** (-0.5)).astype(bf16)
            return carry

        lax.fori_loop(0, q_width // LANES, query_body, 0)

    kv_heads = k_width // HEAD_DIM
    groups = q_width // HEAD_DIM // kv_heads
    span = 3 * WINDOW
    gap = lax.broadcasted_iota(jnp.int32, (WINDOW, span), 1) - lax.broadcasted_iota(
        jnp.int32, (WINDOW, span), 0
    )
    window = (gap >= 0) & (gap <= 2 * WINDOW)

    def attend(i):
        at = pl.ds(pl.multiple_of(i * WINDOW, WINDOW), WINDOW)
        near = pl.ds(pl.multiple_of(i * WINDOW, WINDOW), span)
        allowed = window & (doc_col[at, 0:1] == doc_row[0:1, near])
        bias = jnp.where(allowed, 0.0, -jnp.inf)
        bias = jnp.concatenate([bias] * groups, axis=0)
        queries = query_s[at, :]
        pairs = pair_ext[near, :]
        for head in range(kv_heads):
            keys = pairs[:, head * HEAD_DIM : (head + 1) * HEAD_DIM]
            values = pairs[:, k_width + head * HEAD_DIM : k_width + (head + 1) * HEAD_DIM]
            first = head * groups
            stack = jnp.concatenate(
                [
                    queries[:, (first + g) * HEAD_DIM : (first + g + 1) * HEAD_DIM]
                    for g in range(groups)
                ],
                axis=0,
            )
            sinks = jnp.concatenate(
                [jnp.full((WINDOW, 1), sink_ref[first + g], f32) for g in range(groups)], axis=0
            )
            scores = lax.dot_general(
                stack, keys, (((1,), (1,)), ((), ())), preferred_element_type=f32
            )
            scores = scores + bias
            top = jnp.maximum(jnp.max(scores, axis=1, keepdims=True), sinks)
            expo = jnp.exp(scores - top)
            total = jnp.sum(expo, axis=1, keepdims=True) + jnp.exp(sinks - top)
            weight = (expo * (1.0 / total)).astype(bf16)
            result = jnp.dot(weight, values, preferred_element_type=f32).astype(bf16)
            wide = jnp.concatenate(
                [result[g * WINDOW : (g + 1) * WINDOW] for g in range(groups)], axis=1
            )
            attended[at, first * HEAD_DIM : (first + groups) * HEAD_DIM] = wide

    def attend_all(count, pick):
        begin, lag = state[0], state[1]

        def body(j, carry):
            with jax.named_scope("attend"):
                attend(pick(j))
            with jax.named_scope("att_ev"):
                on(begin + j, z_event)
                on(lag + j, y_event)
                att_copy(pick(j)).start()
            return carry

        lax.fori_loop(0, count, body, 0)
        state[0] += count
        state[1] += count

    def carry_on(k):
        mine = slice(k * CHUNK, (k + 1) * CHUNK)
        ext = slice(edge + k * CHUNK, edge + (k + 1) * CHUNK)
        project(k, 0, 2 * c_width)

        def body(j, carry):
            carried[ext, block(0, j)] = (
                proj_ref[mine, block(0, j)] * proj_ref[mine, block(c_width, j)]
            ).astype(bf16)
            return carry

        lax.fori_loop(0, c_width // LANES, body, 0)

    row_c = lax.broadcasted_iota(jnp.int32, (CHUNK, LANES), 0)

    def convolve(k):
        begin, end = k * CHUNK, (k + 1) * CHUNK
        mine = slice(begin, end)
        project(k, 2 * c_width, k_at)

        def body(j, carry):
            at = block(0, j)
            docs_here = doc_col[mine, :]
            cells = carried[edge + begin : edge + end, at].astype(f32)
            head = carried[begin : begin + edge, at].astype(f32)
            foot = carried[edge + end : 2 * edge + end, at].astype(f32)
            before = jnp.where(row_c == 0, head[edge - 1 : edge, :], pltpu.roll(cells, 1, 0))
            after = jnp.where(row_c == CHUNK - 1, foot[0:1, :], pltpu.roll(cells, CHUNK - 1, 0))
            doc_before = jnp.where(
                row_c == 0,
                doc_row[0:1, WINDOW + begin - 1 : WINDOW + begin],
                pltpu.roll(docs_here, 1, 0),
            )
            doc_after = jnp.where(
                row_c == CHUNK - 1,
                doc_row[0:1, WINDOW + end : WINDOW + end + 1],
                pltpu.roll(docs_here, CHUNK - 1, 0),
            )
            conv = jnp.where(doc_before == docs_here, before * taps_ref[0:1, at], 0.0)
            conv = conv + cells * taps_ref[1:2, at]
            conv = conv + jnp.where(doc_after == docs_here, after * taps_ref[2:3, at], 0.0)
            convolved[mine, at] = (
                proj_ref[mine, block(2 * c_width, j)] * (conv + bias_ref[:, at])
            ).astype(bf16)
            return carry

        lax.fori_loop(0, c_width // LANES, body, 0)

    with jax.named_scope("adv_a"):
        advance(marks[1] - counts[0] + 1)
        start_own(1)
    with jax.named_scope("scale_0"):
        scale(order[0])
    with jax.named_scope("adv_b"):
        advance(marks[1] + 2)
    with jax.named_scope("settle_0"):
        settle(0)
    with jax.named_scope("att_proj_0"):
        project_att(order[0])
        start_halo(1, 0)
    with jax.named_scope("adv_c"):
        advance(marks[1] + 4)
    with jax.named_scope("scale_1"):
        scale(order[1])
    with jax.named_scope("att_proj_1"):
        project_att(order[1])
        start_halo(1, 1)
    with jax.named_scope("adv_d"):
        advance(marks[1] + 5)
        wait_halo(0)
        wait_halo(1)
    attend_all(2, lambda j: j * (blocks - 1))
    with jax.named_scope("adv_e"):
        advance(marks[2] - counts[1] + 1)
        start_own(2)
    for k in order[2:]:
        with jax.named_scope("scale_2"):
            scale(k)
        with jax.named_scope("att_proj_2"):
            project_att(k)
    with jax.named_scope("adv_f"):
        advance(marks[2] - 2)
    attend_all(blocks - 2, lambda j: j + 1)
    with jax.named_scope("settle_1"):
        settle(1)
    with jax.named_scope("carry_0"):
        carry_on(order[0])
    with jax.named_scope("carry_1"):
        carry_on(order[1])
        start_halo(2, 0)
        start_halo(2, 1)
    with jax.named_scope("adv_g"):
        advance(marks[2] + 3)
    for k in order[2:]:
        with jax.named_scope("carry_2"):
            carry_on(k)
    with jax.named_scope("adv_h"):
        advance(marks[2] + 4)
        wait_halo(2)
    for n, k in enumerate(order):
        with jax.named_scope("convolve"):
            convolve(k)
            conv_copy(k).start()
        with jax.named_scope("adv_i"):
            advance(min(marks[3], marks[2] + 5 + n))
    with jax.named_scope("settle_2"):
        settle(2)

    with jax.named_scope("att_wait"):
        for i in range(blocks):
            att_copy(i).wait_recv()
    q_mine = pl.ds(pl.multiple_of(x * q_width, q_width), q_width)
    q_yours = pl.ds(pl.multiple_of((1 - x) * q_width, q_width), q_width)
    c_mine = pl.ds(pl.multiple_of(x * c_width, c_width), c_width)
    c_yours = pl.ds(pl.multiple_of((1 - x) * c_width, c_width), c_width)

    def mix_body(j, carry):
        at = pl.ds(pl.multiple_of(j * cut, cut), cut)
        late = pl.ds(pl.multiple_of(part + j * cut, cut), cut)
        acc = jnp.dot(attended[...], wo_full[q_mine, at], preferred_element_type=f32)
        acc = acc + jnp.dot(att_other[...], wo_full[q_yours, at], preferred_element_type=f32)
        acc = acc + jnp.dot(convolved[...], wo_full[c_mine, late], preferred_element_type=f32)
        acc_ref[:, at] = acc
        return carry

    with jax.named_scope("mix"):
        lax.fori_loop(0, part // cut, mix_body, 0)

    with jax.named_scope("sends"):
        for kind in range(3):
            for way in range(2):

                @pl.when(sends_to[way])
                def _():
                    halo(kind, way).wait_send()

        for i in range(blocks):
            att_copy(i).wait_send()
        for k in range(chunks):
            x_copy(k).wait_send()
        for g in range(3):
            own_d(g, c).wait_send()

            def sent(m, carry):
                t, j = m // counts[g], m % counts[g]
                for way in range(2):

                    @pl.when(has_next[way] & (t < lines - 1) & arrives(way, t))
                    def _():
                        z_copy(way, t, g, j).wait_send()

                    @pl.when((t > 0) & arrives(way, t))
                    def _():
                        y_copy(way, t, g, j).wait_send()
                        d_copy(0, way, t, g, j, c).wait_send()
                        d_copy(1, way, t, g, j, c).wait_send()

                return carry

            lax.fori_loop(0, lines * counts[g], sent, 0)

    def out_copy(k):
        at = slice(k * CHUNK, (k + 1) * CHUNK)
        return pltpu.make_async_copy(stage.at[at, :], out_ref.at[at, :], out_sem.at[k])

    for k in order:
        mine = slice(k * CHUNK, (k + 1) * CHUNK)
        with jax.named_scope("conv_wait"):
            conv_copy(k).wait_recv()

        def last_body(j, carry):
            at = pl.ds(pl.multiple_of(j * cut, cut), cut)
            late = pl.ds(pl.multiple_of(part + j * cut, cut), cut)
            acc = acc_ref[mine, at] + jnp.dot(
                conv_other[mine, :], wo_full[c_yours, late], preferred_element_type=f32
            )
            stage[mine, at] = acc.astype(bf16)
            return carry

        with jax.named_scope("last"):
            lax.fori_loop(0, part // cut, last_body, 0)
            out_copy(k).start()

    with jax.named_scope("end"):
        for k in range(chunks):
            conv_copy(k).wait_send()
        for k in range(chunks):
            out_copy(k).wait()


def fused_layer(
    tokens, gain, projections, outputs, sink_logit, taps, conv_bias, documents, sp_count
):
    rows, part = tokens.shape
    f32 = jnp.float32
    bf16 = jnp.bfloat16
    lines = sp_count // 2
    wk, wv, wc, wu, wb, wq = projections
    width = sum(w.shape[1] for w in projections)
    rp, ro = wq.shape[0], outputs[0].shape[0]
    q_width, k_width, c_width = wq.shape[1], wk.shape[1], wc.shape[1]
    half = HEAD_DIM // 2
    freq = np.power(THETA, -(np.arange(half) / half))
    freq = jnp.asarray(np.tile(freq, LANES // half)[None, :], f32)
    chunks, blocks = rows // CHUNK, rows // WINDOW
    dma = pltpu.SemaphoreType.DMA
    hops = (2, lines - 1, CONV_UNITS + ATT_UNITS + OUT_UNITS)
    vmem = pl.BlockSpec(memory_space=pltpu.VMEM)
    hbm = pl.BlockSpec(memory_space=pl.ANY)
    smem = pl.BlockSpec(memory_space=pltpu.SMEM)
    flops = 2 * rows * 2 * part * width
    return pl.pallas_call(
        functools.partial(layer_kernel, (lines, rp, ro)),
        out_shape=jax.ShapeDtypeStruct((rows, part), bf16),
        in_specs=[hbm, vmem] + [hbm] * 8 + [smem] + [vmem] * 4,
        out_specs=hbm,
        scratch_shapes=[
            pltpu.VMEM((rp * sp_count, width), bf16),
            pltpu.VMEM((ro * sp_count, 2 * part), bf16),
            pltpu.VMEM((rows, part), bf16),
            pltpu.VMEM((rows, part), bf16),
            pltpu.VMEM((rows, 2 * part), bf16),
            pltpu.VMEM((rows, LANES), f32),
            pltpu.VMEM((rows, width), f32),
            pltpu.VMEM((rows, part), f32),
            pltpu.VMEM((rows, part), bf16),
            pltpu.VMEM((rows + 2 * WINDOW, 2 * k_width), bf16),
            pltpu.VMEM((rows, q_width), bf16),
            pltpu.VMEM((rows + 32, c_width), bf16),
            pltpu.VMEM((8, rows + 2 * WINDOW), f32),
            pltpu.VMEM((rows, LANES), f32),
            pltpu.VMEM((64, LANES), f32),
            pltpu.VMEM((rows, LANES), f32),
            pltpu.VMEM((rows, LANES), f32),
            pltpu.VMEM((rows, c_width), bf16),
            pltpu.VMEM((rows, c_width), bf16),
            pltpu.VMEM((rows, q_width), bf16),
            pltpu.VMEM((rows, q_width), bf16),
        ]
        + [dma(hops)] * 8
        + [dma((3,)), dma((3,)), dma((chunks,)), dma((chunks,)), dma((9,)), dma((chunks,))]
        + [dma((chunks,)), dma((3, 2)), dma((3, 2)), dma((chunks,)), dma((chunks,))]
        + [dma((blocks,)), dma((blocks,))],
        compiler_params=pltpu.CompilerParams(
            collective_id=0, has_side_effects=True, vmem_limit_bytes=62 * 1024 * 1024
        ),
        cost_estimate=pl.CostEstimate(flops=flops, bytes_accessed=0, transcendentals=0),
        name="layer",
    )(
        tokens,
        gain[None, :],
        *projections,
        *outputs,
        sink_logit,
        taps,
        conv_bias[None, :],
        documents[None, :],
        freq,
    )


def extended(cells, sides, width):
    for axis, dim in sides:
        count = lax.axis_size(axis)
        ends = count - 1
        head = lax.slice_in_dim(cells, 0, width, axis=dim)
        tail = lax.slice_in_dim(cells, cells.shape[dim] - width, cells.shape[dim], axis=dim)
        cells = jnp.concatenate(
            [
                lax.ppermute(tail, axis, [(i, (i + 1) % count) for i in range(ends)]),
                cells,
                lax.ppermute(head, axis, [((i + 1) % count, i) for i in range(ends)]),
            ],
            axis=dim,
        )
    return cells


def rotate(proj, positions, heads):
    rows = proj.shape[0]
    size = proj.shape[1] // heads
    half = size // 2
    freq = jnp.power(THETA, -(jnp.arange(half, dtype=jnp.float32) * (2.0 / size)))
    angle = positions.astype(jnp.float32)[:, None] * freq[None, :]
    cosine = jnp.cos(angle)[:, None, :]
    sine = jnp.sin(angle)[:, None, :]
    shaped = proj.reshape(rows, heads, size)
    first = shaped[..., :half]
    second = shaped[..., half:]
    turned = jnp.concatenate(
        [first * cosine - second * sine, second * cosine + first * sine], axis=-1
    )
    return turned.reshape(rows, heads * size)


def sink_softmax(scores, allowed, sinks):
    masked = jnp.where(allowed, scores, -jnp.inf)
    top = jnp.maximum(jnp.max(masked, axis=-1, keepdims=True), sinks)
    expo = jnp.exp(masked - top)
    return expo / (jnp.sum(expo, axis=-1, keepdims=True) + jnp.exp(sinks - top))


def local(
    tokens,
    gain,
    w_query,
    w_key,
    w_value,
    w_input,
    w_bgate,
    w_cgate,
    w_attn_out,
    w_conv_out,
    sink_logit,
    taps,
    conv_bias,
    documents,
):
    f32 = jnp.float32
    bf16 = jnp.bfloat16
    rows, part = tokens.shape
    tp_count = lax.axis_size("tp")
    sp_count = lax.axis_size("sp")
    width = part * tp_count
    head_dim = HEAD_DIM
    q_local = w_query.shape[1] // head_dim
    kv_local = w_key.shape[1] // head_dim
    groups = q_local // kv_local
    if fused_plan(
        lax.axis_size("grp"),
        sp_count,
        tp_count,
        rows,
        part,
        w_query.shape[0],
        w_attn_out.shape[0],
        w_query.shape[1],
        w_key.shape[1],
        w_input.shape[1],
    ):
        return fused_layer(
            tokens,
            gain,
            (w_key, w_value, w_cgate, w_input, w_bgate, w_query),
            (w_attn_out, w_conv_out),
            sink_logit,
            taps,
            conv_bias,
            documents,
            sp_count,
        )
    wq, wk, wv, wu, wb, wc, w_attn, w_conv = (
        lax.all_gather(w_query, "sp", axis=0, tiled=True),
        lax.all_gather(w_key, "sp", axis=0, tiled=True),
        lax.all_gather(w_value, "sp", axis=0, tiled=True),
        lax.all_gather(w_input, "sp", axis=0, tiled=True),
        lax.all_gather(w_bgate, "sp", axis=0, tiled=True),
        lax.all_gather(w_cgate, "sp", axis=0, tiled=True),
        lax.all_gather(w_attn_out, "sp", axis=0, tiled=True),
        lax.all_gather(w_conv_out, "sp", axis=0, tiled=True),
    )
    matrices = (wq, wk, wv, wu, wb, wc)
    piece_f = lax.all_gather(tokens, "tp", axis=1, tiled=True).astype(f32)
    scaled = (piece_f * gain[None, :]).astype(bf16)
    products = tuple((jnp.dot(scaled, mat, preferred_element_type=f32) for mat in matrices))
    folded = products + (jnp.sum(piece_f * piece_f, axis=1),)
    sums = folded[:6]
    squares = folded[6]
    inv = lax.rsqrt(squares / width + EPS)[:, None]
    q_acc, k_acc, v_acc, u_acc, b_acc, c_acc = sums
    positions = lax.axis_index("sp") * rows + jnp.arange(rows, dtype=jnp.int32)
    query = rotate(q_acc * inv, positions, q_local).astype(bf16)
    keys = rotate(k_acc * inv, positions, kv_local).astype(bf16)
    values = (v_acc * inv).astype(bf16)
    carried = (c_acc * inv * (u_acc * inv)).astype(bf16)
    bgate = b_acc * inv
    doc_col = documents.astype(f32).astype(bf16)[:, None]
    paired = jnp.concatenate([keys, values], axis=1)
    pair_ext, doc_ext = (
        extended(paired, (("sp", 0),), WINDOW),
        extended(doc_col, (("sp", 0),), WINDOW),
    )
    carry_ext, doc_near = (extended(carried, (("sp", 0),), 1), extended(doc_col, (("sp", 0),), 1))
    key_width = kv_local * head_dim
    key_ext = pair_ext[:, :key_width].reshape(-1, kv_local, head_dim)
    val_ext = pair_ext[:, key_width:].reshape(-1, kv_local, head_dim)
    key_doc = doc_ext[:, 0].astype(f32)
    own_doc = doc_col[:, 0].astype(f32)
    key_pos = positions[0] - WINDOW + jnp.arange(rows + 2 * WINDOW, dtype=jnp.int32)
    total = sp_count * rows
    sinks = sink_logit.reshape(kv_local, groups, 1, 1)
    block = rows // 2
    outputs = []
    for begin in range(0, rows, block):
        span = block + 2 * WINDOW
        q_block = query[begin : begin + block].reshape(block, kv_local, groups, head_dim)
        k_block = key_ext[begin : begin + span]
        v_block = val_ext[begin : begin + span]
        q_pos = positions[begin : begin + block]
        k_pos = key_pos[begin : begin + span]
        scores = jnp.einsum(
            "qhgd,khd->hgqk", q_block, k_block, preferred_element_type=f32
        ) * head_dim ** (-0.5)
        allowed = jnp.abs(q_pos[:, None] - k_pos[None, :]) <= WINDOW
        allowed = allowed & (
            own_doc[begin : begin + block, None] == key_doc[None, begin : begin + span]
        )
        allowed = allowed & (k_pos >= 0)[None, :] & (k_pos < total)[None, :]
        weight = sink_softmax(scores, allowed, sinks).astype(bf16)
        result = jnp.einsum("hgqk,khd->qhgd", weight, v_block, preferred_element_type=f32)
        outputs.append(result.astype(bf16).reshape(block, q_local * head_dim))
    attended = jnp.concatenate(outputs, axis=0)
    near_doc = doc_near[:, 0].astype(f32)
    conv = jnp.zeros((rows, carried.shape[1]), f32)
    for tap in range(3):
        same = (near_doc[tap : tap + rows] == near_doc[1 : rows + 1])[:, None]
        conv = conv + jnp.where(
            same, carry_ext[tap : tap + rows].astype(f32) * taps[tap][None, :], 0.0
        )
    convolved = (bgate * (conv + conv_bias[None, :])).astype(bf16)
    acc = jnp.dot(
        lax.all_gather(attended, "tp", axis=1, tiled=True), w_attn, preferred_element_type=f32
    )
    mixed = acc + jnp.dot(
        lax.all_gather(convolved, "tp", axis=1, tiled=True), w_conv, preferred_element_type=f32
    )
    return mixed.astype(bf16)


def solution(mesh):
    placed = (
        P(("grp", "sp"), "tp"),
        P(),
        P("sp", "tp"),
        P("sp", "tp"),
        P("sp", "tp"),
        P("sp", "tp"),
        P("sp", "tp"),
        P("sp", "tp"),
        P("sp", "tp"),
        P("sp", "tp"),
        P("tp"),
        P(None, "tp"),
        P("tp"),
        P(("grp", "sp")),
    )
    return jax.shard_map(
        local, mesh=mesh, in_specs=placed, out_specs=P(("grp", "sp"), "tp"), check_vma=False
    )
```

time: 109 us -> 99.3 us (0.911)
  Pallas kernels: 100 us -> 95.1 us
  other arithmetic: 3.73 us -> 0 us
    pallas_call x1, Pallas kernels: 100 us -> 95.1 us  [fused_layer(): pl.pallas_call(functools.partial(layer_kernel, (lines, rp, ro)), out_shap...]
    concatenate x1 -> x0, other arithmetic: 1.58 us -> none  [fused_layer(): cosine = jnp.concatenate([cosine] * (lanes // half), axis=1)]
    neg x1 -> x0, other arithmetic: 1.44 us -> none  [fused_layer(): sine = jnp.concatenate([-sine, sine] * (lanes // HEAD_DIM), axis=1)]
where the time goes in v1:
time: 99.3 us; the launch traced here: 99.1 us
  Pallas kernels  95.1 us (96%)
  local copies, waits for them, and re-layouts  3.94 us (4%)
    pallas_call x1, Pallas kernels, fused_layer(): pl.pallas_call(functools.partial(layer_kernel, (lines, rp, ro)), out_shap...  95.1 us
    unnamed x1, local copies, waits for them, and re-layouts  2.67 us

profile of v1, /device:TPU:0, one launch (start us, length us, event | category | flops | bytes accessed | tf_op | source)
XLA Modules:
  0.0 99.1 jit_solution(16734372797916758778)
XLA Ops:
  0.0 1.3 %broadcast_in_dim.11.doc_ref = s32[1,768]{1,0:T(1,128)} reshape(s32[768]{0:T(1024)} %param.28) | data formatting | bytes 6144 | tf_op jit(solution)/shard_map/broadcast_in_dim | solution.py:783
  1.3 95.1 %layer.1 = bf16[768,1024]{1,0:T(8,128)(2,1)} custom-call(bf16[768,1024]{1,0:T(8,128)(2,1)} %tok_hbm.1, f32[1,2048]{1,0:T(1,128)} %bitcast.2, bf16[256,128]{1,0:T(8,128)(2,1)} %wk_ref.1, bf16[256,128]{1,0:T(8,128)(2,1)} %wv_ref.1, bf16[256,512]{1,0:T(8,128)(2,1)} %wc_ref.1, bf16[256,512]{1,0:T(8,128)(2,1)} %wu_ref.1, bf16[256,512]{1,0:T(8,128)(2,1)} %wb_ref.1, ...), custom_call_target="tpu_custom_call" | custom-call | flops 7247757312 | tf_op jit(solution)/shard_map/layer/pallas_call | solution.py:738
  96.4 2.7 %copy.17 = bf16[768,1024]{1,0:T(8,128)(2,1)} copy(bf16[768,1024]{1,0:T(8,128)(2,1)} %layer.1) | data formatting | bytes 3145728

commit v2 on v1

--- a/solution.py
+++ b/solution.py
@@ -14,10 +14,8 @@
 
 EPS = 1e-06
 THETA = 500000.0
-ATT_UNITS = 2
-CONV_UNITS = 4
-OUT_UNITS = 2
-LATE = 3
+UNITS = (4, 4, 4)
+LATES = (6, 3, 4)
 CHUNK = 256
 LANES = 128
 
@@ -29,15 +27,14 @@
         and tp_count == 2
         and sp_count % 2 == 0
         and lines == 4
-        and proj_rows % (2 * CONV_UNITS * 16) == 0
-        and proj_rows % (2 * ATT_UNITS * 16) == 0
-        and out_rows % (2 * OUT_UNITS * 16) == 0
+        and all(proj_rows % (2 * units * 16) == 0 for units in UNITS[:2])
+        and all(out_rows % (2 * units * 16) == 0 for units in UNITS[2:])
         and rows % CHUNK == 0
         and 3 * CHUNK <= rows <= 1024
         and CHUNK == 2 * WINDOW
         and WINDOW == LANES
-        and part % 256 == 0
-        and q_width % 256 == 0
+        and part % 512 == 0
+        and q_width == 4 * k_width
         and k_width == LANES
         and c_width % 256 == 0
         and 2 * HEAD_DIM == LANES
@@ -68,7 +65,6 @@
     tok_other,
     scaled,
     inv_ref,
-    proj_ref,
     acc_ref,
     stage,
     pair_ext,
@@ -87,12 +83,8 @@
     z_recv,
     y_send,
     y_recv,
-    dz_send,
-    dz_recv,
-    dy_send,
-    dy_recv,
-    do_send,
-    do_recv,
+    d_send,
+    d_recv,
     x_send,
     x_recv,
     own_sem,
@@ -120,13 +112,14 @@
     sp = lax.axis_index("sp")
     x = lax.axis_index("tp")
     z, c = sp // 2, sp % 2
-    counts = (ATT_UNITS, CONV_UNITS, OUT_UNITS)
+    counts = UNITS
+    kinds = range(len(counts))
     fulls = (wp_full, wp_full, wo_full)
     heights = (rp, rp, ro)
     spans = ((k_at, width), (0, k_at), (0, 2 * part))
-    first_unit = (0, ATT_UNITS, ATT_UNITS + CONV_UNITS)
-    marks = [0]
+    first_unit, marks = [0], [0]
     for count in counts:
+        first_unit.append(first_unit[-1] + count)
         marks.append(marks[-1] + (lines - 1) * count)
     to_y = {"grp": 1 - y}
     to_core = {"sp": z * 2 + 1 - c}
@@ -153,44 +146,41 @@
         )
 
     def z_copy(way, t, g, j):
-        ref, u = place(g, j, origin(way, t), c, y), first_unit[g] + j
-        return remote(ref, ref, z_send.at[way, t, u], z_recv.at[way, t, u], to_z[way])
-
-    def z_arrival(way, t, g, j):
-        ref, u = place(g, j, origin(way, t), c, y), first_unit[g] + j
-        return remote(ref, ref, z_send.at[way, t - 1, u], z_recv.at[way, t - 1, u], to_z[way])
-
-    def y_copy(way, t, g, j):
-        ref, u = place(g, j, origin(way, t), c, y), first_unit[g] + j
-        return remote(ref, ref, y_send.at[way, t - 1, u], y_recv.at[way, t - 1, u], to_y)
-
-    def y_arrival(way, t, g, j):
-        ref, u = place(g, j, origin(way, t), c, 1 - y), first_unit[g] + j
-        return remote(ref, ref, y_send.at[way, t - 1, u], y_recv.at[way, t - 1, u], to_y)
-
-    def d_copy(kind, way, t, g, j, cc):
-        send, recv = (dz_send, dz_recv) if kind == 0 else (dy_send, dy_recv)
-        ref, u = place(g, j, origin(way, t), cc, y if kind == 0 else 1 - y), first_unit[g] + j
-        return remote(ref, ref, send.at[way, t - 1, u], recv.at[way, t - 1, u], to_core)
-
-    def own_rows(g, cc):
-        size = heights[g]
-        return pl.ds(pl.multiple_of((z * 2 + cc) * size, size), size)
-
-    def own_d(g, cc):
-        dst = fulls[g].at[own_rows(g, cc), spans[g][0] : spans[g][1]]
-        return remote(dst, dst, do_send.at[g], do_recv.at[g], to_core)
+        zo = origin(way, t)
+        ref, u = place(g, j, zo, c, y), first_unit[g] + j
+        return remote(ref, ref, z_send.at[way, g], z_recv.at[zo - way, u], to_z[way])
+
+    def y_copy(way, t, g, j, h):
+        zo = origin(way, t)
+        ref, u = place(g, j, zo, c, h), first_unit[g] + j
+        return remote(ref, ref, y_send.at[g], y_recv.at[zo - way, u], to_y)
+
+    def d_copy(way, t, g, j, h):
+        ref = place(g, j, origin(way, t), c, h)
+        return remote(ref, ref, d_send.at[g], d_recv.at[g], to_core)
+
+    def some_rows(g, count):
+        return fulls[g].at[0:count, spans[g][0] : spans[g][1]]
+
+    def d_all(g, shards):
+        ref = some_rows(g, shards * heights[g])
+        return remote(ref, ref, d_send.at[g], d_recv.at[g], to_core)
+
+    def own_ref(g):
+        at = pl.ds(pl.multiple_of((z * 2 + c) * heights[g], heights[g]), heights[g])
+        return fulls[g].at[at, spans[g][0] : spans[g][1]]
+
+    def own_d(g):
+        return remote(own_ref(g), own_ref(g), d_send.at[g], d_recv.at[g], to_core)
 
     own_refs = ((wk_ref, wv_ref, wq_ref), (wc_ref, wu_ref, wb_ref), (wa_ref, wm_ref))
 
     def own_local(g):
-        at, copies, col = own_rows(g, c), [], spans[g][0]
-        for j, ref in enumerate(own_refs[g]):
+        at, copies, col = pl.ds(pl.multiple_of((z * 2 + c) * heights[g], heights[g]), heights[g]), [], spans[g][0]
+        for ref in own_refs[g]:
             size = ref.shape[1]
             copies.append(
-                pltpu.make_async_copy(
-                    ref, fulls[g].at[at, col : col + size], own_sem.at[3 * g + j]
-                )
+                pltpu.make_async_copy(ref, fulls[g].at[at, col : col + size], own_sem.at[g])
             )
             col += size
         return copies
@@ -201,7 +191,7 @@
 
     def x_copy(k):
         at = slice(k * CHUNK, (k + 1) * CHUNK)
-        return remote(tok_own.at[at, :], tok_other.at[at, :], x_send.at[k], x_recv.at[k], to_x)
+        return remote(tok_own.at[at, :], tok_other.at[at, :], x_send.at[0], x_recv.at[k], to_x)
 
     last = 2 * lines - 1
     steps_sp = (sp + 1, sp - 1)
@@ -246,16 +236,15 @@
     def conv_copy(k):
         at = slice(k * CHUNK, (k + 1) * CHUNK)
         return remote(
-            convolved.at[at, :], conv_other.at[at, :], conv_send.at[k], conv_recv.at[k], to_x
+            convolved.at[at, :], conv_other.at[at, :], conv_send.at[0], conv_recv.at[k], to_x
         )
 
     def att_copy(i):
         at = pl.ds(pl.multiple_of(i * WINDOW, WINDOW), WINDOW)
-        return remote(attended.at[at, :], att_other.at[at, :], att_send.at[i], att_recv.at[i], to_x)
+        return remote(attended.at[at, :], att_other.at[at, :], att_send.at[0], att_recv.at[i], to_x)
 
     def start_own(g):
-        for copy in own_local(g):
-            copy.wait()
+        pltpu.make_async_copy(own_ref(g), own_ref(g), own_sem.at[g]).wait()
         for j in range(counts[g]):
             for way in range(2):
 
@@ -263,7 +252,7 @@
                 def _():
                     z_copy(way, 0, g, j).start()
 
-        own_d(g, c).start()
+        own_d(g).start()
 
     def z_event(g, m):
         t, j = m // counts[g] + 1, m % counts[g]
@@ -271,14 +260,14 @@
 
             @pl.when(arrives(way, t))
             def _():
-                z_arrival(way, t, g, j).wait_recv()
+                z_copy(way, t, g, j).wait_recv()
 
                 @pl.when(has_next[way] & (t < lines - 1))
                 def _():
                     z_copy(way, t, g, j).start()
 
-                y_copy(way, t, g, j).start()
-                d_copy(0, way, t, g, j, c).start()
+                y_copy(way, t, g, j, y).start()
+                d_copy(way, t, g, j, y).start()
 
     def y_event(g, m):
         t, j = m // counts[g] + 1, m % counts[g]
@@ -286,27 +275,32 @@
 
             @pl.when(arrives(way, t))
             def _():
-                y_arrival(way, t, g, j).wait_recv()
-                d_copy(1, way, t, g, j, c).start()
+                y_copy(way, t, g, j, 1 - y).wait_recv()
+                d_copy(way, t, g, j, 1 - y).start()
 
     def on(n, act):
         if isinstance(n, int):
-            g = max(i for i in range(3) if marks[i] <= n)
+            g = max(i for i in kinds if marks[i] <= n)
             act(g, n - marks[g])
             return
-        for g in range(3):
+        for g in kinds:
 
             @pl.when((n >= marks[g]) & (n < marks[g + 1]))
             def _():
                 act(g, n - marks[g])
 
     state = [0, 0]
+
+    def due(m):
+        if m >= marks[-1]:
+            return m
+        return m + LATES[max(i for i in kinds if marks[i] <= m)]
 
     def advance(goal):
         while state[0] < goal:
             on(state[0], z_event)
             state[0] += 1
-            while state[1] < state[0] - LATE:
+            while due(state[1]) < state[0]:
                 on(state[1], y_event)
                 state[1] += 1
 
@@ -315,24 +309,11 @@
         while state[1] < marks[g + 1]:
             on(state[1], y_event)
             state[1] += 1
-        own_d(g, 1 - c).wait_recv()
-
-        def arrived(m, carry):
-            t, j = m // counts[g] + 1, m % counts[g]
-            for way in range(2):
-
-                @pl.when(arrives(way, t))
-                def _():
-                    d_copy(0, way, t, g, j, 1 - c).wait_recv()
-                    d_copy(1, way, t, g, j, 1 - c).wait_recv()
-
-            return carry
-
-        lax.fori_loop(0, marks[g + 1] - marks[g], arrived, 0)
+        d_all(g, lines).wait_recv()
 
     for k in order:
         tok_local(k).start()
-    for g in range(3):
+    for g in kinds:
         for copy in own_local(g):
             copy.start()
 
@@ -354,7 +335,10 @@
         )
 
     docs = doc_ref[...].astype(f32)
-    doc_row[:, WINDOW : WINDOW + rows] = jnp.broadcast_to(docs, (doc_row.shape[0], rows))
+    for i in range(blocks):
+        doc_row[:, (i + 1) * WINDOW : (i + 2) * WINDOW] = jnp.broadcast_to(
+            docs[i : i + 1, :], (doc_row.shape[0], LANES)
+        )
 
     @pl.when(sp == 0)
     def _():
@@ -379,7 +363,7 @@
 
     for i in range(blocks):
         at = slice(i * WINDOW, (i + 1) * WINDOW)
-        doc_col[at, :] = jnp.broadcast_to(docs[:, at], (WINDOW, LANES)).T
+        doc_col[at, :] = jnp.broadcast_to(docs[i : i + 1, :], (WINDOW, LANES)).T
 
     tile = 32
     lane = lax.broadcasted_iota(jnp.int32, (tile, LANES), 1)
@@ -427,42 +411,43 @@
 
     cut = 256
 
-    def project(k, begin, end):
+    def project(k, at):
         mine = slice(k * CHUNK, (k + 1) * CHUNK)
-
-        def body(j, carry):
-            at = pl.ds(pl.multiple_of(j * cut, cut), cut)
-            acc = jnp.dot(scaled[mine, :], wp_full[:, at], preferred_element_type=f32)
-            proj_ref[mine, at] = acc * inv_ref[mine, :1]
-            return carry
-
-        lax.fori_loop(begin // cut, end // cut, body, 0)
+        acc = jnp.dot(scaled[mine, :], wp_full[:, at], preferred_element_type=f32)
+        return acc * inv_ref[mine, :1]
 
     lane_c = lax.broadcasted_iota(jnp.int32, (CHUNK, LANES), 1)
     low = (lane_c % HEAD_DIM) < HEAD_DIM // 2
-
-    def block(at, j):
-        return pl.ds(pl.multiple_of(at + j * LANES, LANES), LANES)
+    left = lane_c < HEAD_DIM
 
     def project_att(k):
         mine = slice(k * CHUNK, (k + 1) * CHUNK)
         ext = slice(WINDOW + k * CHUNK, WINDOW + (k + 1) * CHUNK)
-        project(k, k_at, width)
 
         def turned(cells):
             ahead = pltpu.roll(cells, LANES - HEAD_DIM // 2, 1)
             behind = pltpu.roll(cells, HEAD_DIM // 2, 1)
             return cells * cos_ref[mine, :] + jnp.where(low, ahead, behind) * sin_ref[mine, :]
 
-        pair_ext[ext, :k_width] = turned(proj_ref[mine, k_at : k_at + k_width]).astype(bf16)
-        pair_ext[ext, k_width:] = proj_ref[mine, k_at + k_width : q_at].astype(bf16)
+        cells = project(k, slice(k_at, q_at))
+        pair_ext[ext, :k_width] = turned(cells[:, :k_width]).astype(bf16)
+        pair_ext[ext, k_width:] = cells[:, k_width:].astype(bf16)
 
         def query_body(j, carry):
-            cells = turned(proj_ref[mine, block(q_at, j)])
-            query_s[mine, block(0, j)] = (cells * HEAD_DIM ** (-0.5)).astype(bf16)
+            cells = project(k, pl.ds(pl.multiple_of(q_at + j * cut, cut), cut))
+            for i in range(cut // LANES):
+                pair = turned(cells[:, i * LANES : (i + 1) * LANES]) * HEAD_DIM ** (-0.5)
+                swapped = pltpu.roll(pair, HEAD_DIM, 1)
+                own_half = left == (j == 0)
+                first = jnp.where(own_half, jnp.where(j == 0, pair, swapped), 0.0)
+                second = jnp.where(own_half, jnp.where(j == 0, swapped, pair), 0.0)
+                at = pl.multiple_of((j * (cut // LANES) + i) * 2 * LANES, LANES)
+                query_s[mine, pl.ds(at, LANES)] = first.astype(bf16)
+                query_s[mine, pl.ds(at + LANES, LANES)] = second.astype(bf16)
             return carry
 
-        lax.fori_loop(0, q_width // LANES, query_body, 0)
+        for j in range(q_width // cut):
+            query_body(j, 0)
 
     kv_heads = k_width // HEAD_DIM
     groups = q_width // HEAD_DIM // kv_heads
@@ -471,6 +456,7 @@
         jnp.int32, (WINDOW, span), 0
     )
     window = (gap >= 0) & (gap <= 2 * WINDOW)
+    left_w = left[:WINDOW, :]
 
     def attend(i):
         at = pl.ds(pl.multiple_of(i * WINDOW, WINDOW), WINDOW)
@@ -478,15 +464,15 @@
         allowed = window & (doc_col[at, 0:1] == doc_row[0:1, near])
         bias = jnp.where(allowed, 0.0, -jnp.inf)
         bias = jnp.concatenate([bias] * groups, axis=0)
-        queries = query_s[at, :]
-        pairs = pair_ext[near, :]
+        keys = pair_ext[near, :k_width]
+        values = jnp.concatenate(
+            [pair_ext[near, k_width:], jnp.ones((span, LANES), bf16)], axis=1
+        )
         for head in range(kv_heads):
-            keys = pairs[:, head * HEAD_DIM : (head + 1) * HEAD_DIM]
-            values = pairs[:, k_width + head * HEAD_DIM : k_width + (head + 1) * HEAD_DIM]
             first = head * groups
             stack = jnp.concatenate(
                 [
-                    queries[:, (first + g) * HEAD_DIM : (first + g + 1) * HEAD_DIM]
+                    query_s[at, (first + g) * LANES : (first + g + 1) * LANES]
                     for g in range(groups)
                 ],
                 axis=0,
@@ -499,14 +485,19 @@
             )
             scores = scores + bias
             top = jnp.maximum(jnp.max(scores, axis=1, keepdims=True), sinks)
-            expo = jnp.exp(scores - top)
-            total = jnp.sum(expo, axis=1, keepdims=True) + jnp.exp(sinks - top)
-            weight = (expo * (1.0 / total)).astype(bf16)
-            result = jnp.dot(weight, values, preferred_element_type=f32).astype(bf16)
-            wide = jnp.concatenate(
-                [result[g * WINDOW : (g + 1) * WINDOW] for g in range(groups)], axis=1
-            )
-            attended[at, first * HEAD_DIM : (first + groups) * HEAD_DIM] = wide
+            expo = jnp.exp(scores - top).astype(bf16)
+            result = jnp.dot(expo, values, preferred_element_type=f32)
+            total = result[:, LANES:] + jnp.exp(sinks - top)
+            result = result[:, :LANES] * (1.0 / total)
+            for g in range(0, groups, 2):
+                one = result[g * WINDOW : (g + 1) * WINDOW]
+                two = result[(g + 1) * WINDOW : (g + 2) * WINDOW]
+                if head == 0:
+                    pair = jnp.where(left_w, one, pltpu.roll(two, HEAD_DIM, 1))
+                else:
+                    pair = jnp.where(left_w, pltpu.roll(one, HEAD_DIM, 1), two)
+                to = (first + g) * HEAD_DIM
+                attended[at, to : to + LANES] = pair.astype(bf16)
 
     def attend_all(count, pick):
         begin, lag = state[0], state[1]
@@ -525,56 +516,57 @@
         state[1] += count
 
     def carry_on(k):
-        mine = slice(k * CHUNK, (k + 1) * CHUNK)
         ext = slice(edge + k * CHUNK, edge + (k + 1) * CHUNK)
-        project(k, 0, 2 * c_width)
-
-        def body(j, carry):
-            carried[ext, block(0, j)] = (
-                proj_ref[mine, block(0, j)] * proj_ref[mine, block(c_width, j)]
+        for j in range(c_width // cut):
+            at = slice(j * cut, (j + 1) * cut)
+            gate = project(k, at)
+            carried[ext, at] = (
+                gate * project(k, slice(c_width + j * cut, c_width + (j + 1) * cut))
             ).astype(bf16)
-            return carry
-
-        lax.fori_loop(0, c_width // LANES, body, 0)
 
     row_c = lax.broadcasted_iota(jnp.int32, (CHUNK, LANES), 0)
 
     def convolve(k):
         begin, end = k * CHUNK, (k + 1) * CHUNK
         mine = slice(begin, end)
-        project(k, 2 * c_width, k_at)
-
-        def body(j, carry):
-            at = block(0, j)
-            docs_here = doc_col[mine, :]
-            cells = carried[edge + begin : edge + end, at].astype(f32)
-            head = carried[begin : begin + edge, at].astype(f32)
-            foot = carried[edge + end : 2 * edge + end, at].astype(f32)
-            before = jnp.where(row_c == 0, head[edge - 1 : edge, :], pltpu.roll(cells, 1, 0))
-            after = jnp.where(row_c == CHUNK - 1, foot[0:1, :], pltpu.roll(cells, CHUNK - 1, 0))
-            doc_before = jnp.where(
-                row_c == 0,
-                doc_row[0:1, WINDOW + begin - 1 : WINDOW + begin],
-                pltpu.roll(docs_here, 1, 0),
-            )
-            doc_after = jnp.where(
-                row_c == CHUNK - 1,
-                doc_row[0:1, WINDOW + end : WINDOW + end + 1],
-                pltpu.roll(docs_here, CHUNK - 1, 0),
-            )
-            conv = jnp.where(doc_before == docs_here, before * taps_ref[0:1, at], 0.0)
-            conv = conv + cells * taps_ref[1:2, at]
-            conv = conv + jnp.where(doc_after == docs_here, after * taps_ref[2:3, at], 0.0)
-            convolved[mine, at] = (
-                proj_ref[mine, block(2 * c_width, j)] * (conv + bias_ref[:, at])
-            ).astype(bf16)
-            return carry
-
-        lax.fori_loop(0, c_width // LANES, body, 0)
+        docs_here = doc_col[mine, :]
+        doc_before = jnp.where(
+            row_c == 0,
+            doc_row[0:1, WINDOW + begin - 1 : WINDOW + begin],
+            pltpu.roll(docs_here, 1, 0),
+        )
+        doc_after = jnp.where(
+            row_c == CHUNK - 1,
+            doc_row[0:1, WINDOW + end : WINDOW + end + 1],
+            pltpu.roll(docs_here, CHUNK - 1, 0),
+        )
+        for j in range(c_width // cut):
+            gates = project(k, slice(2 * c_width + j * cut, 2 * c_width + (j + 1) * cut))
+            for i in range(cut // LANES):
+                at = slice(j * cut + i * LANES, j * cut + (i + 1) * LANES)
+                cells = carried[edge + begin : edge + end, at].astype(f32)
+                head = carried[begin : begin + edge, at].astype(f32)
+                foot = carried[edge + end : 2 * edge + end, at].astype(f32)
+                before = jnp.where(row_c == 0, head[edge - 1 : edge, :], pltpu.roll(cells, 1, 0))
+                after = jnp.where(row_c == CHUNK - 1, foot[0:1, :], pltpu.roll(cells, CHUNK - 1, 0))
+                conv = jnp.where(doc_before == docs_here, before * taps_ref[0:1, at], 0.0)
+                conv = conv + cells * taps_ref[1:2, at]
+                conv = conv + jnp.where(doc_after == docs_here, after * taps_ref[2:3, at], 0.0)
+                gate = gates[:, i * LANES : (i + 1) * LANES]
+                convolved[mine, at] = (gate * (conv + bias_ref[:, at])).astype(bf16)
+
+    def ahead_of(g):
+        return marks[g + 1] - counts[g] + 1
+
+    q_mine = pl.ds(pl.multiple_of(x * q_width, q_width), q_width)
+    q_yours = pl.ds(pl.multiple_of((1 - x) * q_width, q_width), q_width)
+    c_mine = pl.ds(pl.multiple_of(x * c_width, c_width), c_width)
+    c_yours = pl.ds(pl.multiple_of((1 - x) * c_width, c_width), c_width)
 
     with jax.named_scope("adv_a"):
-        advance(marks[1] - counts[0] + 1)
+        advance(ahead_of(0))
         start_own(1)
+        advance(marks[1] - 1)
     with jax.named_scope("scale_0"):
         scale(order[0])
     with jax.named_scope("adv_b"):
@@ -592,12 +584,12 @@
         project_att(order[1])
         start_halo(1, 1)
     with jax.named_scope("adv_d"):
-        advance(marks[1] + 5)
+        advance(marks[1] + 6)
         wait_halo(0)
         wait_halo(1)
     attend_all(2, lambda j: j * (blocks - 1))
     with jax.named_scope("adv_e"):
-        advance(marks[2] - counts[1] + 1)
+        advance(ahead_of(1))
         start_own(2)
     for k in order[2:]:
         with jax.named_scope("scale_2"):
@@ -605,40 +597,38 @@
         with jax.named_scope("att_proj_2"):
             project_att(k)
     with jax.named_scope("adv_f"):
-        advance(marks[2] - 2)
+        advance(marks[2] - 1)
     attend_all(blocks - 2, lambda j: j + 1)
     with jax.named_scope("settle_1"):
         settle(1)
     with jax.named_scope("carry_0"):
         carry_on(order[0])
+    with jax.named_scope("adv_g"):
+        advance(marks[2] + 4)
     with jax.named_scope("carry_1"):
         carry_on(order[1])
         start_halo(2, 0)
         start_halo(2, 1)
-    with jax.named_scope("adv_g"):
-        advance(marks[2] + 3)
+    with jax.named_scope("adv_g2"):
+        advance(marks[2] + 5)
     for k in order[2:]:
         with jax.named_scope("carry_2"):
             carry_on(k)
     with jax.named_scope("adv_h"):
-        advance(marks[2] + 4)
+        advance(marks[2] + 6)
         wait_halo(2)
     for n, k in enumerate(order):
         with jax.named_scope("convolve"):
             convolve(k)
             conv_copy(k).start()
         with jax.named_scope("adv_i"):
-            advance(min(marks[3], marks[2] + 5 + n))
+            advance(min(marks[3], marks[2] + 7 + n))
     with jax.named_scope("settle_2"):
         settle(2)
 
     with jax.named_scope("att_wait"):
         for i in range(blocks):
             att_copy(i).wait_recv()
-    q_mine = pl.ds(pl.multiple_of(x * q_width, q_width), q_width)
-    q_yours = pl.ds(pl.multiple_of((1 - x) * q_width, q_width), q_width)
-    c_mine = pl.ds(pl.multiple_of(x * c_width, c_width), c_width)
-    c_yours = pl.ds(pl.multiple_of((1 - x) * c_width, c_width), c_width)
 
     def mix_body(j, carry):
         at = pl.ds(pl.multiple_of(j * cut, cut), cut)
@@ -660,58 +650,45 @@
                 def _():
                     halo(kind, way).wait_send()
 
-        for i in range(blocks):
-            att_copy(i).wait_send()
-        for k in range(chunks):
-            x_copy(k).wait_send()
-        for g in range(3):
-            own_d(g, c).wait_send()
-
-            def sent(m, carry):
-                t, j = m // counts[g], m % counts[g]
-                for way in range(2):
-
-                    @pl.when(has_next[way] & (t < lines - 1) & arrives(way, t))
+        for g in kinds:
+            d_all(g, lines).wait_send()
+            ref = some_rows(g, (lines - 1) * heights[g] // 2)
+            remote(ref, ref, y_send.at[g], y_recv.at[0, 0], to_y).wait_send()
+            for way in range(2):
+                for shards in range(1, lines):
+
+                    @pl.when((z + 1 if way == 0 else lines - z) == shards)
                     def _():
-                        z_copy(way, t, g, j).wait_send()
-
-                    @pl.when((t > 0) & arrives(way, t))
-                    def _():
-                        y_copy(way, t, g, j).wait_send()
-                        d_copy(0, way, t, g, j, c).wait_send()
-                        d_copy(1, way, t, g, j, c).wait_send()
-
-                return carry
-
-            lax.fori_loop(0, lines * counts[g], sent, 0)
+                        ref = some_rows(g, shards * heights[g] // 2)
+                        remote(ref, ref, z_send.at[way, g], z_recv.at[0, 0], to_z[way]).wait_send()
+
+        remote(tok_own, tok_other, x_send.at[0], x_recv.at[0], to_x).wait_send()
+        remote(attended, att_other, att_send.at[0], att_recv.at[0], to_x).wait_send()
 
     def out_copy(k):
         at = slice(k * CHUNK, (k + 1) * CHUNK)
-        return pltpu.make_async_copy(stage.at[at, :], out_ref.at[at, :], out_sem.at[k])
-
+        return pltpu.make_async_copy(stage.at[at, :], out_ref.at[at, :], out_sem.at[0])
+
+    wide = 512
     for k in order:
         mine = slice(k * CHUNK, (k + 1) * CHUNK)
         with jax.named_scope("conv_wait"):
             conv_copy(k).wait_recv()
 
-        def last_body(j, carry):
-            at = pl.ds(pl.multiple_of(j * cut, cut), cut)
-            late = pl.ds(pl.multiple_of(part + j * cut, cut), cut)
-            acc = acc_ref[mine, at] + jnp.dot(
-                conv_other[mine, :], wo_full[c_yours, late], preferred_element_type=f32
-            )
-            stage[mine, at] = acc.astype(bf16)
-            return carry
-
         with jax.named_scope("last"):
-            lax.fori_loop(0, part // cut, last_body, 0)
+            for j in range(part // wide):
+                at = slice(j * wide, (j + 1) * wide)
+                acc = acc_ref[mine, at] + jnp.dot(
+                    conv_other[mine, :],
+                    wo_full[c_yours, part + j * wide : part + (j + 1) * wide],
+                    preferred_element_type=f32,
+                )
+                stage[mine, at] = acc.astype(bf16)
             out_copy(k).start()
 
     with jax.named_scope("end"):
-        for k in range(chunks):
-            conv_copy(k).wait_send()
-        for k in range(chunks):
-            out_copy(k).wait()
+        remote(convolved, conv_other, conv_send.at[0], conv_recv.at[0], to_x).wait_send()
+        pltpu.make_async_copy(stage, out_ref, out_sem.at[0]).wait()
 
 
 def fused_layer(
@@ -730,7 +707,8 @@
     freq = jnp.asarray(np.tile(freq, LANES // half)[None, :], f32)
     chunks, blocks = rows // CHUNK, rows // WINDOW
     dma = pltpu.SemaphoreType.DMA
-    hops = (2, lines - 1, CONV_UNITS + ATT_UNITS + OUT_UNITS)
+    hops = (lines - 1, sum(UNITS))
+    kinds = len(UNITS)
     vmem = pl.BlockSpec(memory_space=pltpu.VMEM)
     hbm = pl.BlockSpec(memory_space=pl.ANY)
     smem = pl.BlockSpec(memory_space=pltpu.SMEM)
@@ -747,11 +725,10 @@
             pltpu.VMEM((rows, part), bf16),
             pltpu.VMEM((rows, 2 * part), bf16),
             pltpu.VMEM((rows, LANES), f32),
-            pltpu.VMEM((rows, width), f32),
             pltpu.VMEM((rows, part), f32),
             pltpu.VMEM((rows, part), bf16),
             pltpu.VMEM((rows + 2 * WINDOW, 2 * k_width), bf16),
-            pltpu.VMEM((rows, q_width), bf16),
+            pltpu.VMEM((rows, 2 * q_width), bf16),
             pltpu.VMEM((rows + 32, c_width), bf16),
             pltpu.VMEM((8, rows + 2 * WINDOW), f32),
             pltpu.VMEM((rows, LANES), f32),
@@ -763,10 +740,9 @@
             pltpu.VMEM((rows, q_width), bf16),
             pltpu.VMEM((rows, q_width), bf16),
         ]
-        + [dma(hops)] * 8
-        + [dma((3,)), dma((3,)), dma((chunks,)), dma((chunks,)), dma((9,)), dma((chunks,))]
-        + [dma((chunks,)), dma((3, 2)), dma((3, 2)), dma((chunks,)), dma((chunks,))]
-        + [dma((blocks,)), dma((blocks,))],
+        + [dma((2, kinds)), dma(hops), dma((kinds,)), dma(hops), dma((kinds,)), dma((kinds,))]
+        + [dma((1,)), dma((chunks,)), dma((kinds,)), dma((chunks,)), dma((1,))]
+        + [dma((3, 2)), dma((3, 2)), dma((1,)), dma((chunks,)), dma((1,)), dma((blocks,))],
         compiler_params=pltpu.CompilerParams(
             collective_id=0, has_side_effects=True, vmem_limit_bytes=62 * 1024 * 1024
         ),
@@ -780,7 +756,7 @@
         sink_logit,
         taps,
         conv_bias[None, :],
-        documents[None, :],
+        documents.reshape(blocks, LANES),
         freq,
     )
 

time: 99.3 us -> 83.7 us (0.84)
  Pallas kernels: 95.1 us -> 80.8 us
  local copies, waits for them, and re-layouts: 3.94 us -> 2.67 us
    pallas_call x1, Pallas kernels: 95.1 us -> 80.8 us  [fused_layer(): pl.pallas_call(functools.partial(layer_kernel, (lines, rp, ro)), out_shap...]
    broadcast_in_dim x1 -> x0, local copies, waits for them, and re-layouts: 1.27 us -> none  [fused_layer(): documents[None, :]]
where the time goes in v2:
time: 83.7 us; the launch traced here: 83.5 us
  Pallas kernels  80.8 us (97%)
  local copies, waits for them, and re-layouts  2.67 us (3%)
    pallas_call x1, Pallas kernels, fused_layer(): pl.pallas_call(functools.partial(layer_kernel, (lines, rp, ro)), out_shap...  80.8 us
    unnamed x1, local copies, waits for them, and re-layouts  2.67 us

profile of v2, /device:TPU:0, one launch (start us, length us, event | category | flops | bytes accessed | tf_op | source)
XLA Modules:
  0.0 83.5 jit_solution(723782427241304460)
XLA Ops:
  0.0 80.8 %layer.1 = bf16[768,1024]{1,0:T(8,128)(2,1)} custom-call(bf16[768,1024]{1,0:T(8,128)(2,1)} %tok_hbm.1, f32[1,2048]{1,0:T(1,128)} %bitcast.3, bf16[256,128]{1,0:T(8,128)(2,1)} %wk_ref.1, bf16[256,128]{1,0:T(8,128)(2,1)} %wv_ref.1, bf16[256,512]{1,0:T(8,128)(2,1)} %wc_ref.1, bf16[256,512]{1,0:T(8,128)(2,1)} %wu_ref.1, bf16[256,512]{1,0:T(8,128)(2,1)} %wb_ref.1, ...), custom_call_target="tpu_custom_call" | custom-call | flops 7247757312 | tf_op jit(solution)/shard_map/layer/pallas_call | solution.py:716
  80.8 2.7 %copy.17 = bf16[768,1024]{1,0:T(8,128)(2,1)} copy(bf16[768,1024]{1,0:T(8,128)(2,1)} %layer.1) | data formatting | bytes 3145728

commit v3 on v2

--- a/solution.py
+++ b/solution.py
@@ -14,8 +14,8 @@
 
 EPS = 1e-06
 THETA = 500000.0
-UNITS = (4, 4, 4)
-LATES = (6, 3, 4)
+UNITS = (4, 4, 4, 4)
+LAGS = (7, 6, 8, 6)
 CHUNK = 256
 LANES = 128
 
@@ -27,8 +27,8 @@
         and tp_count == 2
         and sp_count % 2 == 0
         and lines == 4
-        and all(proj_rows % (2 * units * 16) == 0 for units in UNITS[:2])
-        and all(out_rows % (2 * units * 16) == 0 for units in UNITS[2:])
+        and all(proj_rows % (2 * units * 16) == 0 for units in UNITS[:3])
+        and all(out_rows % (2 * units * 16) == 0 for units in UNITS[3:])
         and rows % CHUNK == 0
         and 3 * CHUNK <= rows <= 1024
         and CHUNK == 2 * WINDOW
@@ -44,7 +44,7 @@
 def layer_kernel(
     sizes,
     tok_hbm,
-    gain_ref,
+    gain_hbm,
     wk_ref,
     wv_ref,
     wc_ref,
@@ -53,12 +53,18 @@
     wq_ref,
     wa_ref,
     wm_ref,
+    sink_hbm,
+    taps_hbm,
+    bias_hbm,
+    doc_hbm,
+    freq_hbm,
+    out_ref,
+    gain_ref,
     sink_ref,
     taps_ref,
     bias_ref,
     doc_ref,
     freq_ref,
-    out_ref,
     wp_full,
     wo_full,
     tok_own,
@@ -66,7 +72,6 @@
     scaled,
     inv_ref,
     acc_ref,
-    stage,
     pair_ext,
     query_s,
     carried,
@@ -89,7 +94,7 @@
     x_recv,
     own_sem,
     tok_sem,
-    out_sem,
+    small_sem,
     halo_send,
     halo_recv,
     conv_send,
@@ -108,15 +113,17 @@
     chunks = rows // CHUNK
     blocks = rows // WINDOW
     order = (chunks - 1,) + tuple(range(chunks - 1))
+    pieces = [(k * CHUNK, CHUNK) for k in order[:-1]]
+    pieces += [(order[-1] * CHUNK, WINDOW), (order[-1] * CHUNK + WINDOW, WINDOW)]
     y = lax.axis_index("grp")
     sp = lax.axis_index("sp")
     x = lax.axis_index("tp")
     z, c = sp // 2, sp % 2
     counts = UNITS
     kinds = range(len(counts))
-    fulls = (wp_full, wp_full, wo_full)
-    heights = (rp, rp, ro)
-    spans = ((k_at, width), (0, k_at), (0, 2 * part))
+    fulls = (wp_full, wp_full, wp_full, wo_full)
+    heights = (rp, rp, rp, ro)
+    spans = ((k_at, width), (0, 2 * c_width), (2 * c_width, k_at), (0, 2 * part))
     first_unit, marks = [0], [0]
     for count in counts:
         first_unit.append(first_unit[-1] + count)
@@ -173,7 +180,7 @@
     def own_d(g):
         return remote(own_ref(g), own_ref(g), d_send.at[g], d_recv.at[g], to_core)
 
-    own_refs = ((wk_ref, wv_ref, wq_ref), (wc_ref, wu_ref, wb_ref), (wa_ref, wm_ref))
+    own_refs = ((wk_ref, wv_ref, wq_ref), (wc_ref, wu_ref), (wb_ref,), (wa_ref, wm_ref))
 
     def own_local(g):
         at, copies, col = pl.ds(pl.multiple_of((z * 2 + c) * heights[g], heights[g]), heights[g]), [], spans[g][0]
@@ -185,13 +192,13 @@
             col += size
         return copies
 
-    def tok_local(k):
-        at = slice(k * CHUNK, (k + 1) * CHUNK)
-        return pltpu.make_async_copy(tok_hbm.at[at, :], tok_own.at[at, :], tok_sem.at[k])
-
-    def x_copy(k):
-        at = slice(k * CHUNK, (k + 1) * CHUNK)
-        return remote(tok_own.at[at, :], tok_other.at[at, :], x_send.at[0], x_recv.at[k], to_x)
+    def tok_local(i):
+        at = slice(pieces[i][0], sum(pieces[i]))
+        return pltpu.make_async_copy(tok_hbm.at[at, :], tok_own.at[at, :], tok_sem.at[i])
+
+    def x_copy(i):
+        at = slice(pieces[i][0], sum(pieces[i]))
+        return remote(tok_own.at[at, :], tok_other.at[at, :], x_send.at[0], x_recv.at[i], to_x)
 
     last = 2 * lines - 1
     steps_sp = (sp + 1, sp - 1)
@@ -226,12 +233,10 @@
         def _():
             halo(kind, way).start()
 
-    def wait_halo(kind):
-        for way in range(2):
-
-            @pl.when(gets_from[way])
-            def _():
-                halo(kind, way).wait_recv()
+    def wait_halo(kind, way):
+        @pl.when(gets_from[way])
+        def _():
+            halo(kind, way).wait_recv()
 
     def conv_copy(k):
         at = slice(k * CHUNK, (k + 1) * CHUNK)
@@ -291,10 +296,15 @@
 
     state = [0, 0]
 
+    costs = [heights[g] // counts[g] * (spans[g][1] - spans[g][0]) for g in kinds]
+    unit_of = [g for g in kinds for _ in range((lines - 1) * counts[g])]
+    ends = [sum(costs[g] for g in unit_of[: n + 1]) for n in range(marks[-1])]
+
     def due(m):
         if m >= marks[-1]:
             return m
-        return m + LATES[max(i for i in kinds if marks[i] <= m)]
+        limit = ends[m] + LAGS[unit_of[m]] * costs[unit_of[m]]
+        return max(n for n in range(marks[-1]) if ends[n] <= limit)
 
     def advance(goal):
         while state[0] < goal:
@@ -304,19 +314,29 @@
                 on(state[1], y_event)
                 state[1] += 1
 
-    def settle(g):
-        advance(marks[g + 1])
+    def flush(g):
         while state[1] < marks[g + 1]:
             on(state[1], y_event)
             state[1] += 1
+
+    def settle(g):
+        advance(marks[g + 1])
+        flush(g)
         d_all(g, lines).wait_recv()
 
-    for k in order:
-        tok_local(k).start()
-    for g in kinds:
-        for copy in own_local(g):
-            copy.start()
-
+    small = [
+        pltpu.make_async_copy(src, dst, small_sem.at[i])
+        for i, (src, dst) in enumerate(
+            (
+                (doc_hbm, doc_ref),
+                (freq_hbm, freq_ref),
+                (gain_hbm, gain_ref),
+                (taps_hbm, taps_ref),
+                (bias_hbm, bias_ref),
+                (sink_hbm, sink_ref),
+            )
+        )
+    ]
     barrier = pltpu.get_barrier_semaphore()
     for device in (to_y, to_core, to_x):
         pl.semaphore_signal(barrier, inc=1, device_id=device, device_id_type=pl.DeviceIdType.MESH)
@@ -334,6 +354,14 @@
             barrier, inc=1, device_id={"sp": side}, device_id_type=pl.DeviceIdType.MESH
         )
 
+    for i in range(len(pieces)):
+        tok_local(i).start()
+    for g in kinds:
+        for copy in own_local(g):
+            copy.start()
+    for copy in small:
+        copy.start()
+    small[0].wait()
     docs = doc_ref[...].astype(f32)
     for i in range(blocks):
         doc_row[:, (i + 1) * WINDOW : (i + 2) * WINDOW] = jnp.broadcast_to(
@@ -354,9 +382,9 @@
     with jax.named_scope("barrier"):
         pl.semaphore_wait(barrier, neighbours)
 
-    for k in order:
-        tok_local(k).wait()
-        x_copy(k).start()
+    for i in range(len(pieces)):
+        tok_local(i).wait()
+        x_copy(i).start()
     start_own(0)
     for way in range(2):
         start_halo(0, way)
@@ -368,6 +396,8 @@
     tile = 32
     lane = lax.broadcasted_iota(jnp.int32, (tile, LANES), 1)
     step = lax.broadcasted_iota(jnp.int32, (tile, LANES), 0)
+    for copy in small[1:]:
+        copy.wait()
     freq = freq_ref[...]
     far = (sp * rows + step * tile).astype(f32) * freq
     near_angle = step.astype(f32) * freq
@@ -388,11 +418,12 @@
     mine_at = pl.multiple_of(x * part, part)
     yours_at = pl.multiple_of((1 - x) * part, part)
 
-    def scale(k):
-        x_copy(k).wait_recv()
+    def scale(piece):
+        begin, size = pieces[piece]
+        x_copy(piece).wait_recv()
 
         def body(i, carry):
-            at = pl.ds(pl.multiple_of(k * CHUNK + i * tile, tile), tile)
+            at = pl.ds(pl.multiple_of(begin + i * tile, tile), tile)
             own = tok_own[at, :].astype(f32)
             other = tok_other[at, :].astype(f32)
             total = jnp.sum(own * own, axis=1, keepdims=True) + jnp.sum(
@@ -407,12 +438,11 @@
             ).astype(bf16)
             return carry
 
-        lax.fori_loop(0, CHUNK // tile, body, 0)
+        lax.fori_loop(0, size // tile, body, 0)
 
     cut = 256
 
-    def project(k, at):
-        mine = slice(k * CHUNK, (k + 1) * CHUNK)
+    def project(mine, at):
         acc = jnp.dot(scaled[mine, :], wp_full[:, at], preferred_element_type=f32)
         return acc * inv_ref[mine, :1]
 
@@ -420,25 +450,26 @@
     low = (lane_c % HEAD_DIM) < HEAD_DIM // 2
     left = lane_c < HEAD_DIM
 
-    def project_att(k):
-        mine = slice(k * CHUNK, (k + 1) * CHUNK)
-        ext = slice(WINDOW + k * CHUNK, WINDOW + (k + 1) * CHUNK)
+    def project_att(piece):
+        begin, size = pieces[piece]
+        mine = slice(begin, begin + size)
+        ext = slice(WINDOW + begin, WINDOW + begin + size)
 
         def turned(cells):
             ahead = pltpu.roll(cells, LANES - HEAD_DIM // 2, 1)
             behind = pltpu.roll(cells, HEAD_DIM // 2, 1)
-            return cells * cos_ref[mine, :] + jnp.where(low, ahead, behind) * sin_ref[mine, :]
-
-        cells = project(k, slice(k_at, q_at))
+            return cells * cos_ref[mine, :] + jnp.where(low[:size], ahead, behind) * sin_ref[mine, :]
+
+        cells = project(mine, slice(k_at, q_at))
         pair_ext[ext, :k_width] = turned(cells[:, :k_width]).astype(bf16)
         pair_ext[ext, k_width:] = cells[:, k_width:].astype(bf16)
 
         def query_body(j, carry):
-            cells = project(k, pl.ds(pl.multiple_of(q_at + j * cut, cut), cut))
+            cells = project(mine, pl.ds(pl.multiple_of(q_at + j * cut, cut), cut))
             for i in range(cut // LANES):
                 pair = turned(cells[:, i * LANES : (i + 1) * LANES]) * HEAD_DIM ** (-0.5)
                 swapped = pltpu.roll(pair, HEAD_DIM, 1)
-                own_half = left == (j == 0)
+                own_half = left[:size] == (j == 0)
                 first = jnp.where(own_half, jnp.where(j == 0, pair, swapped), 0.0)
                 second = jnp.where(own_half, jnp.where(j == 0, swapped, pair), 0.0)
                 at = pl.multiple_of((j * (cut // LANES) + i) * 2 * LANES, LANES)
@@ -499,29 +530,39 @@
                 to = (first + g) * HEAD_DIM
                 attended[at, to : to + LANES] = pair.astype(bf16)
 
-    def attend_all(count, pick):
-        begin, lag = state[0], state[1]
+    def attend_all(count, events, pick, guard=False):
+        begin, lag = state
 
         def body(j, carry):
+            if guard:
+                with jax.named_scope("halo_wait"):
+                    for way in range(2):
+
+                        @pl.when(gets_from[way] & (j == way))
+                        def _():
+                            halo(1, way).wait_recv()
+
             with jax.named_scope("attend"):
                 attend(pick(j))
+                att_copy(pick(j)).start()
             with jax.named_scope("att_ev"):
-                on(begin + j, z_event)
-                on(lag + j, y_event)
-                att_copy(pick(j)).start()
+                for e in range(events):
+                    on(begin + j * events + e, z_event)
+                    on(lag + j * events + e, y_event)
             return carry
 
         lax.fori_loop(0, count, body, 0)
-        state[0] += count
-        state[1] += count
+        state[0] += count * events
+        state[1] += count * events
 
     def carry_on(k):
+        mine = slice(k * CHUNK, (k + 1) * CHUNK)
         ext = slice(edge + k * CHUNK, edge + (k + 1) * CHUNK)
         for j in range(c_width // cut):
             at = slice(j * cut, (j + 1) * cut)
-            gate = project(k, at)
+            gate = project(mine, at)
             carried[ext, at] = (
-                gate * project(k, slice(c_width + j * cut, c_width + (j + 1) * cut))
+                gate * project(mine, slice(c_width + j * cut, c_width + (j + 1) * cut))
             ).astype(bf16)
 
     row_c = lax.broadcasted_iota(jnp.int32, (CHUNK, LANES), 0)
@@ -541,7 +582,7 @@
             pltpu.roll(docs_here, CHUNK - 1, 0),
         )
         for j in range(c_width // cut):
-            gates = project(k, slice(2 * c_width + j * cut, 2 * c_width + (j + 1) * cut))
+            gates = project(mine, slice(2 * c_width + j * cut, 2 * c_width + (j + 1) * cut))
             for i in range(cut // LANES):
                 at = slice(j * cut + i * LANES, j * cut + (i + 1) * LANES)
                 cells = carried[edge + begin : edge + end, at].astype(f32)
@@ -568,63 +609,83 @@
         start_own(1)
         advance(marks[1] - 1)
     with jax.named_scope("scale_0"):
-        scale(order[0])
+        scale(0)
     with jax.named_scope("adv_b"):
-        advance(marks[1] + 2)
+        advance(marks[1] + 3)
     with jax.named_scope("settle_0"):
         settle(0)
     with jax.named_scope("att_proj_0"):
-        project_att(order[0])
+        project_att(0)
         start_halo(1, 0)
     with jax.named_scope("adv_c"):
-        advance(marks[1] + 4)
+        advance(marks[1] + 7)
     with jax.named_scope("scale_1"):
-        scale(order[1])
+        for i in range(1, len(pieces) - 2):
+            scale(i)
     with jax.named_scope("att_proj_1"):
-        project_att(order[1])
+        project_att(1)
         start_halo(1, 1)
+        for i in range(2, len(pieces) - 2):
+            project_att(i)
     with jax.named_scope("adv_d"):
-        advance(marks[1] + 6)
-        wait_halo(0)
-        wait_halo(1)
-    attend_all(2, lambda j: j * (blocks - 1))
-    with jax.named_scope("adv_e"):
         advance(ahead_of(1))
         start_own(2)
-    for k in order[2:]:
-        with jax.named_scope("scale_2"):
-            scale(k)
-        with jax.named_scope("att_proj_2"):
-            project_att(k)
-    with jax.named_scope("adv_f"):
-        advance(marks[2] - 1)
-    attend_all(blocks - 2, lambda j: j + 1)
+        wait_halo(0, 0)
+        wait_halo(0, 1)
+    attend_all(2, 1, lambda j: j * (blocks - 1), True)
+    with jax.named_scope("adv_e"):
+        advance(marks[2] + 2)
+    with jax.named_scope("scale_2"):
+        scale(len(pieces) - 2)
+    with jax.named_scope("att_proj_2"):
+        project_att(len(pieces) - 2)
+    with jax.named_scope("adv_e2"):
+        advance(marks[2] + 5)
+    attend_all(blocks - 5, 1, lambda j: j + 1)
+    with jax.named_scope("scale_3"):
+        scale(len(pieces) - 1)
+    with jax.named_scope("adv_e3"):
+        advance(marks[2] + 8)
+        start_own(3)
+    with jax.named_scope("att_proj_3"):
+        project_att(len(pieces) - 1)
+    attend_all(2, 2, lambda j: j + blocks - 4)
+    attend_all(1, 0, lambda j: j + blocks - 2)
     with jax.named_scope("settle_1"):
         settle(1)
     with jax.named_scope("carry_0"):
         carry_on(order[0])
-    with jax.named_scope("adv_g"):
-        advance(marks[2] + 4)
+        start_halo(2, 0)
+    with jax.named_scope("adv_f"):
+        advance(marks[3] + 1)
     with jax.named_scope("carry_1"):
         carry_on(order[1])
-        start_halo(2, 0)
         start_halo(2, 1)
-    with jax.named_scope("adv_g2"):
-        advance(marks[2] + 5)
+    with jax.named_scope("adv_h"):
+        advance(marks[3] + 2)
+        flush(2)
     for k in order[2:]:
         with jax.named_scope("carry_2"):
             carry_on(k)
-    with jax.named_scope("adv_h"):
-        advance(marks[2] + 6)
-        wait_halo(2)
-    for n, k in enumerate(order):
+    with jax.named_scope("adv_i"):
+        advance(marks[3] + 3)
+    with jax.named_scope("settle_2"):
+        settle(2)
+    for k in range(chunks):
+        with jax.named_scope("halo_2"):
+            if k == 0:
+                wait_halo(2, 0)
+            if k == chunks - 1:
+                wait_halo(2, 1)
         with jax.named_scope("convolve"):
             convolve(k)
             conv_copy(k).start()
-        with jax.named_scope("adv_i"):
-            advance(min(marks[3], marks[2] + 7 + n))
-    with jax.named_scope("settle_2"):
-        settle(2)
+        with jax.named_scope("adv_j"):
+            advance(min(marks[4], marks[3] + 4 + k))
+    with jax.named_scope("adv_k"):
+        advance(marks[4])
+    with jax.named_scope("settle_3"):
+        settle(3)
 
     with jax.named_scope("att_wait"):
         for i in range(blocks):
@@ -665,12 +726,8 @@
         remote(tok_own, tok_other, x_send.at[0], x_recv.at[0], to_x).wait_send()
         remote(attended, att_other, att_send.at[0], att_recv.at[0], to_x).wait_send()
 
-    def out_copy(k):
-        at = slice(k * CHUNK, (k + 1) * CHUNK)
-        return pltpu.make_async_copy(stage.at[at, :], out_ref.at[at, :], out_sem.at[0])
-
     wide = 512
-    for k in order:
+    for k in range(chunks):
         mine = slice(k * CHUNK, (k + 1) * CHUNK)
         with jax.named_scope("conv_wait"):
             conv_copy(k).wait_recv()
@@ -683,12 +740,10 @@
                     wo_full[c_yours, part + j * wide : part + (j + 1) * wide],
                     preferred_element_type=f32,
                 )
-                stage[mine, at] = acc.astype(bf16)
-            out_copy(k).start()
+                out_ref[mine, at] = acc.astype(bf16)
 
     with jax.named_scope("end"):
         remote(convolved, conv_other, conv_send.at[0], conv_recv.at[0], to_x).wait_send()
-        pltpu.make_async_copy(stage, out_ref, out_sem.at[0]).wait()
 
 
 def fused_layer(
@@ -711,14 +766,19 @@
     kinds = len(UNITS)
     vmem = pl.BlockSpec(memory_space=pltpu.VMEM)
     hbm = pl.BlockSpec(memory_space=pl.ANY)
-    smem = pl.BlockSpec(memory_space=pltpu.SMEM)
     flops = 2 * rows * 2 * part * width
     return pl.pallas_call(
         functools.partial(layer_kernel, (lines, rp, ro)),
-        out_shape=jax.ShapeDtypeStruct((rows, part), bf16),
-        in_specs=[hbm, vmem] + [hbm] * 8 + [smem] + [vmem] * 4,
-        out_specs=hbm,
+        out_shape=pltpu.VMEM((rows, part), bf16),
+        in_specs=[hbm] * 15,
+        out_specs=vmem,
         scratch_shapes=[
+            pltpu.VMEM((1, 2 * part), f32),
+            pltpu.SMEM(sink_logit.shape, f32),
+            pltpu.VMEM(taps.shape, f32),
+            pltpu.VMEM((1, c_width), f32),
+            pltpu.VMEM((blocks, LANES), jnp.int32),
+            pltpu.VMEM((1, LANES), f32),
             pltpu.VMEM((rp * sp_count, width), bf16),
             pltpu.VMEM((ro * sp_count, 2 * part), bf16),
             pltpu.VMEM((rows, part), bf16),
@@ -726,7 +786,6 @@
             pltpu.VMEM((rows, 2 * part), bf16),
             pltpu.VMEM((rows, LANES), f32),
             pltpu.VMEM((rows, part), f32),
-            pltpu.VMEM((rows, part), bf16),
             pltpu.VMEM((rows + 2 * WINDOW, 2 * k_width), bf16),
             pltpu.VMEM((rows, 2 * q_width), bf16),
             pltpu.VMEM((rows + 32, c_width), bf16),
@@ -741,7 +800,7 @@
             pltpu.VMEM((rows, q_width), bf16),
         ]
         + [dma((2, kinds)), dma(hops), dma((kinds,)), dma(hops), dma((kinds,)), dma((kinds,))]
-        + [dma((1,)), dma((chunks,)), dma((kinds,)), dma((chunks,)), dma((1,))]
+        + [dma((1,)), dma((chunks + 1,)), dma((kinds,)), dma((chunks + 1,)), dma((6,))]
         + [dma((3, 2)), dma((3, 2)), dma((1,)), dma((chunks,)), dma((1,)), dma((blocks,))],
         compiler_params=pltpu.CompilerParams(
             collective_id=0, has_side_effects=True, vmem_limit_bytes=62 * 1024 * 1024

time: 83.7 us -> 76.1 us (0.909)
  Pallas kernels: 80.8 us -> 74.8 us
  local copies, waits for them, and re-layouts: 2.67 us -> 1.15 us
    pallas_call x1, Pallas kernels: 80.8 us -> 74.8 us  [fused_layer(): pl.pallas_call(functools.partial(layer_kernel, (lines, rp, ro)), out_shap...]
    unnamed x1, local copies, waits for them, and re-layouts: 2.67 us -> 1.15 us
where the time goes in v3:
time: 76.1 us; the launch traced here: 75.9 us
  Pallas kernels  74.8 us (98%)
  local copies, waits for them, and re-layouts  1.15 us (2%)
    pallas_call x1, Pallas kernels, fused_layer(): pl.pallas_call(functools.partial(layer_kernel, (lines, rp, ro)), out_shap...  74.8 us

profile of v3, /device:TPU:0, one launch (start us, length us, event | category | flops | bytes accessed | tf_op | source)
XLA Modules:
  0.0 75.9 jit_solution(8749788080985204452)
XLA Ops:
  0.0 74.8 %layer.1 = bf16[768,1024]{1,0:T(8,128)(2,1)S(1)} custom-call(bf16[768,1024]{1,0:T(8,128)(2,1)} %tok_hbm.1, f32[1,2048]{1,0:T(1,128)} %bitcast.3, bf16[256,128]{1,0:T(8,128)(2,1)} %wk_ref.1, bf16[256,128]{1,0:T(8,128)(2,1)} %wv_ref.1, bf16[256,512]{1,0:T(8,128)(2,1)} %wc_ref.1, bf16[256,512]{1,0:T(8,128)(2,1)} %wu_ref.1, bf16[256,512]{1,0:T(8,128)(2,1)} %wb_ref.1, ...), custom_call_target="tpu_custom_call" | custom-call | flops 7247757312 | tf_op jit(solution)/shard_map/layer/pallas_call | solution.py:770
  74.8 1.1 %copy.17 = bf16[768,1024]{1,0:T(8,128)(2,1)} copy(bf16[768,1024]{1,0:T(8,128)(2,1)S(1)} %layer.1) | data formatting | bytes 3145728

commit v4 on v3

--- a/solution.py
+++ b/solution.py
@@ -28,7 +28,9 @@
         and sp_count % 2 == 0
         and lines == 4
         and all(proj_rows % (2 * units * 16) == 0 for units in UNITS[:3])
-        and all(out_rows % (2 * units * 16) == 0 for units in UNITS[3:])
+        and UNITS[3] % 2 == 0
+        and UNITS[3] <= UNITS[0]
+        and out_rows % (UNITS[3] * 16) == 0
         and rows % CHUNK == 0
         and 3 * CHUNK <= rows <= 1024
         and CHUNK == 2 * WINDOW
@@ -124,9 +126,8 @@
     fulls = (wp_full, wp_full, wp_full, wo_full)
     heights = (rp, rp, rp, ro)
     spans = ((k_at, width), (0, 2 * c_width), (2 * c_width, k_at), (0, 2 * part))
-    first_unit, marks = [0], [0]
+    first_unit, marks = (0, counts[0], counts[0] + counts[1], 0), [0]
     for count in counts:
-        first_unit.append(first_unit[-1] + count)
         marks.append(marks[-1] + (lines - 1) * count)
     to_y = {"grp": 1 - y}
     to_core = {"sp": z * 2 + 1 - c}
@@ -140,11 +141,24 @@
     def arrives(way, t):
         return z >= t if way == 0 else z < lines - t
 
+    halves = counts[-1] // 2
+
     def place(g, j, zo, cc, h):
         size = heights[g]
-        tall = size // 2 // counts[g]
-        row = (zo * 2 + cc) * size + h * (size // 2) + j * tall
-        return fulls[g].at[pl.ds(pl.multiple_of(row, tall), tall), spans[g][0] : spans[g][1]]
+        row = (zo * 2 + cc) * size + h * (size // 2)
+        if g < 3:
+            tall = size // 2 // counts[g]
+            row = row + j * tall
+            return fulls[g].at[pl.ds(pl.multiple_of(row, tall), tall), spans[g][0] : spans[g][1]]
+        tall = size // 2 // halves
+        row = row + j % halves * tall
+        col = j // halves * part
+        return fulls[g].at[
+            pl.ds(pl.multiple_of(row, tall), tall), pl.ds(pl.multiple_of(col, part), part)
+        ]
+
+    def slot(g, j):
+        return g if g < 3 else 3 + j // halves
 
     def remote(src, dst, send, recv, device):
         return pltpu.make_async_remote_copy(
@@ -155,30 +169,33 @@
     def z_copy(way, t, g, j):
         zo = origin(way, t)
         ref, u = place(g, j, zo, c, y), first_unit[g] + j
-        return remote(ref, ref, z_send.at[way, g], z_recv.at[zo - way, u], to_z[way])
+        return remote(ref, ref, z_send.at[way, g // 3], z_recv.at[zo - way, u], to_z[way])
 
     def y_copy(way, t, g, j, h):
         zo = origin(way, t)
         ref, u = place(g, j, zo, c, h), first_unit[g] + j
-        return remote(ref, ref, y_send.at[g], y_recv.at[zo - way, u], to_y)
+        return remote(ref, ref, y_send.at[g // 3], y_recv.at[zo - way, u], to_y)
 
     def d_copy(way, t, g, j, h):
         ref = place(g, j, origin(way, t), c, h)
-        return remote(ref, ref, d_send.at[g], d_recv.at[g], to_core)
-
-    def some_rows(g, count):
-        return fulls[g].at[0:count, spans[g][0] : spans[g][1]]
-
-    def d_all(g, shards):
-        ref = some_rows(g, shards * heights[g])
-        return remote(ref, ref, d_send.at[g], d_recv.at[g], to_core)
-
-    def own_ref(g):
+        return remote(ref, ref, d_send.at[g // 3], d_recv.at[slot(g, j)], to_core)
+
+    def d_all(n):
+        at = slice(n % 3 * part, (n % 3 + 1) * part) if n >= 3 else slice(*spans[n])
+        g = min(n, 3)
+        ref = fulls[g].at[0 : lines * heights[g], at]
+        return remote(ref, ref, d_send.at[g // 3], d_recv.at[n], to_core)
+
+    def own_wait(full, size):
+        ref = full.at[pl.ds(pl.multiple_of((z * 2 + c) * size, size), size), :]
+        pltpu.make_async_copy(ref, ref, own_sem.at[0 if full is wp_full else 1]).wait()
+
+    def own_d(n):
+        g = min(n, 3)
         at = pl.ds(pl.multiple_of((z * 2 + c) * heights[g], heights[g]), heights[g])
-        return fulls[g].at[at, spans[g][0] : spans[g][1]]
-
-    def own_d(g):
-        return remote(own_ref(g), own_ref(g), d_send.at[g], d_recv.at[g], to_core)
+        cols = slice(n % 3 * part, (n % 3 + 1) * part) if n >= 3 else slice(*spans[n])
+        ref = fulls[g].at[at, cols]
+        return remote(ref, ref, d_send.at[g // 3], d_recv.at[n], to_core)
 
     own_refs = ((wk_ref, wv_ref, wq_ref), (wc_ref, wu_ref), (wb_ref,), (wa_ref, wm_ref))
 
@@ -187,14 +204,14 @@
         for ref in own_refs[g]:
             size = ref.shape[1]
             copies.append(
-                pltpu.make_async_copy(ref, fulls[g].at[at, col : col + size], own_sem.at[g])
+                pltpu.make_async_copy(ref, fulls[g].at[at, col : col + size], own_sem.at[g // 3])
             )
             col += size
         return copies
 
     def tok_local(i):
         at = slice(pieces[i][0], sum(pieces[i]))
-        return pltpu.make_async_copy(tok_hbm.at[at, :], tok_own.at[at, :], tok_sem.at[i])
+        return pltpu.make_async_copy(tok_hbm.at[at, :], tok_own.at[at, :], tok_sem.at[0])
 
     def x_copy(i):
         at = slice(pieces[i][0], sum(pieces[i]))
@@ -238,18 +255,22 @@
         def _():
             halo(kind, way).wait_recv()
 
-    def conv_copy(k):
-        at = slice(k * CHUNK, (k + 1) * CHUNK)
+    tails = [(k * CHUNK, CHUNK) for k in range(chunks - 1)]
+    tails += [(rows - CHUNK, WINDOW), (rows - WINDOW, WINDOW)]
+
+    def conv_copy(i):
+        at = slice(tails[i][0], sum(tails[i]))
         return remote(
-            convolved.at[at, :], conv_other.at[at, :], conv_send.at[0], conv_recv.at[k], to_x
+            convolved.at[at, :], conv_other.at[at, :], conv_send.at[0], conv_recv.at[i], to_x
         )
 
     def att_copy(i):
         at = pl.ds(pl.multiple_of(i * WINDOW, WINDOW), WINDOW)
-        return remote(attended.at[at, :], att_other.at[at, :], att_send.at[0], att_recv.at[i], to_x)
+        return remote(attended.at[at, :], att_other.at[at, :], att_send.at[0], att_recv.at[0], to_x)
 
     def start_own(g):
-        pltpu.make_async_copy(own_ref(g), own_ref(g), own_sem.at[g]).wait()
+        if g == 0 or g == 3:
+            own_wait(fulls[g], heights[g])
         for j in range(counts[g]):
             for way in range(2):
 
@@ -258,6 +279,8 @@
                     z_copy(way, 0, g, j).start()
 
         own_d(g).start()
+        if g == 3:
+            own_d(4).start()
 
     def z_event(g, m):
         t, j = m // counts[g] + 1, m % counts[g]
@@ -304,6 +327,8 @@
         if m >= marks[-1]:
             return m
         limit = ends[m] + LAGS[unit_of[m]] * costs[unit_of[m]]
+        if limit > ends[-1]:
+            return marks[-1]
         return max(n for n in range(marks[-1]) if ends[n] <= limit)
 
     def advance(goal):
@@ -314,29 +339,22 @@
                 on(state[1], y_event)
                 state[1] += 1
 
-    def flush(g):
-        while state[1] < marks[g + 1]:
+    def flush_to(goal):
+        while state[1] < goal:
             on(state[1], y_event)
             state[1] += 1
+
+    def flush(g):
+        flush_to(marks[g + 1])
 
     def settle(g):
         advance(marks[g + 1])
         flush(g)
-        d_all(g, lines).wait_recv()
-
-    small = [
-        pltpu.make_async_copy(src, dst, small_sem.at[i])
-        for i, (src, dst) in enumerate(
-            (
-                (doc_hbm, doc_ref),
-                (freq_hbm, freq_ref),
-                (gain_hbm, gain_ref),
-                (taps_hbm, taps_ref),
-                (bias_hbm, bias_ref),
-                (sink_hbm, sink_ref),
-            )
-        )
-    ]
+        d_all(g).wait_recv()
+
+    def small(src, dst, i):
+        return pltpu.make_async_copy(src, dst, small_sem.at[i])
+
     barrier = pltpu.get_barrier_semaphore()
     for device in (to_y, to_core, to_x):
         pl.semaphore_signal(barrier, inc=1, device_id=device, device_id_type=pl.DeviceIdType.MESH)
@@ -359,9 +377,20 @@
     for g in kinds:
         for copy in own_local(g):
             copy.start()
-    for copy in small:
-        copy.start()
-    small[0].wait()
+    small(doc_hbm, doc_ref, 0).start()
+    small(freq_hbm, freq_ref, 1).start()
+    neighbours = jnp.where(has_side, 1, 0) + jnp.where(z > 0, 1, 0) + jnp.where(z < lines - 1, 1, 0) + 3
+    with jax.named_scope("barrier"):
+        pl.semaphore_wait(barrier, neighbours)
+
+    pltpu.make_async_copy(tok_own, tok_own, tok_sem.at[0]).wait()
+    for i in range(len(pieces)):
+        x_copy(i).start()
+    start_own(0)
+    small(doc_hbm, doc_ref, 0).wait()
+    small(gain_hbm, gain_ref, 0).start()
+    small(freq_hbm, freq_ref, 1).wait()
+    small(taps_hbm, taps_ref, 1).start()
     docs = doc_ref[...].astype(f32)
     for i in range(blocks):
         doc_row[:, (i + 1) * WINDOW : (i + 2) * WINDOW] = jnp.broadcast_to(
@@ -378,17 +407,6 @@
         doc_row[:, WINDOW + rows :] = jnp.full((doc_row.shape[0], WINDOW), -1.0, f32)
         pair_ext[WINDOW + rows :, :] = jnp.zeros((WINDOW, pair_ext.shape[1]), bf16)
 
-    neighbours = jnp.where(has_side, 1, 0) + jnp.where(z > 0, 1, 0) + jnp.where(z < lines - 1, 1, 0) + 3
-    with jax.named_scope("barrier"):
-        pl.semaphore_wait(barrier, neighbours)
-
-    for i in range(len(pieces)):
-        tok_local(i).wait()
-        x_copy(i).start()
-    start_own(0)
-    for way in range(2):
-        start_halo(0, way)
-
     for i in range(blocks):
         at = slice(i * WINDOW, (i + 1) * WINDOW)
         doc_col[at, :] = jnp.broadcast_to(docs[i : i + 1, :], (WINDOW, LANES)).T
@@ -396,8 +414,6 @@
     tile = 32
     lane = lax.broadcasted_iota(jnp.int32, (tile, LANES), 1)
     step = lax.broadcasted_iota(jnp.int32, (tile, LANES), 0)
-    for copy in small[1:]:
-        copy.wait()
     freq = freq_ref[...]
     far = (sp * rows + step * tile).astype(f32) * freq
     near_angle = step.astype(f32) * freq
@@ -414,6 +430,14 @@
         return carry
 
     lax.fori_loop(0, rows // tile, table_body, 0)
+    for way in range(2):
+        start_halo(0, way)
+    small(gain_hbm, gain_ref, 0).wait()
+    small(bias_hbm, bias_ref, 0).start()
+    small(taps_hbm, taps_ref, 1).wait()
+    small(sink_hbm, sink_ref, 1).start()
+    small(bias_hbm, bias_ref, 0).wait()
+    small(sink_hbm, sink_ref, 1).wait()
 
     mine_at = pl.multiple_of(x * part, part)
     yours_at = pl.multiple_of((1 - x) * part, part)
@@ -680,28 +704,45 @@
         with jax.named_scope("convolve"):
             convolve(k)
             conv_copy(k).start()
+            if k == chunks - 1:
+                conv_copy(chunks).start()
         with jax.named_scope("adv_j"):
             advance(min(marks[4], marks[3] + 4 + k))
     with jax.named_scope("adv_k"):
         advance(marks[4])
+        flush_to(marks[4] - counts[3] + halves)
     with jax.named_scope("settle_3"):
-        settle(3)
-
+        d_all(3).wait_recv()
     with jax.named_scope("att_wait"):
-        for i in range(blocks):
-            att_copy(i).wait_recv()
-
-    def mix_body(j, carry):
+        remote(attended, att_other, att_send.at[0], att_recv.at[0], to_x).wait_recv()
+
+    def mix(begin, end):
+        for j in range(begin, end):
+            at = slice(j * cut, (j + 1) * cut)
+            acc = jnp.dot(attended[...], wo_full[q_mine, at], preferred_element_type=f32)
+            acc = acc + jnp.dot(att_other[...], wo_full[q_yours, at], preferred_element_type=f32)
+            acc_ref[:, at] = acc
+
+    cuts = part // cut
+    for j in range(cuts):
+        with jax.named_scope("mix"):
+            mix(j, j + 1)
+        with jax.named_scope("mix_ev"):
+            flush_to(marks[4] - counts[3] + halves + (j + 1) * halves // cuts)
+    with jax.named_scope("settle_4"):
+        flush(3)
+        d_all(4).wait_recv()
+
+    def more_body(j, carry):
         at = pl.ds(pl.multiple_of(j * cut, cut), cut)
         late = pl.ds(pl.multiple_of(part + j * cut, cut), cut)
-        acc = jnp.dot(attended[...], wo_full[q_mine, at], preferred_element_type=f32)
-        acc = acc + jnp.dot(att_other[...], wo_full[q_yours, at], preferred_element_type=f32)
-        acc = acc + jnp.dot(convolved[...], wo_full[c_mine, late], preferred_element_type=f32)
-        acc_ref[:, at] = acc
+        acc_ref[:, at] = acc_ref[:, at] + jnp.dot(
+            convolved[...], wo_full[c_mine, late], preferred_element_type=f32
+        )
         return carry
 
-    with jax.named_scope("mix"):
-        lax.fori_loop(0, part // cut, mix_body, 0)
+    with jax.named_scope("more"):
+        lax.fori_loop(0, cuts, more_body, 0)
 
     with jax.named_scope("sends"):
         for kind in range(3):
@@ -711,26 +752,27 @@
                 def _():
                     halo(kind, way).wait_send()
 
-        for g in kinds:
-            d_all(g, lines).wait_send()
-            ref = some_rows(g, (lines - 1) * heights[g] // 2)
-            remote(ref, ref, y_send.at[g], y_recv.at[0, 0], to_y).wait_send()
+        for n, (full, size) in enumerate(((wp_full, rp), (wo_full, ro))):
+            ref = full.at[0 : lines * size, :]
+            remote(ref, ref, d_send.at[n], d_recv.at[0], to_core).wait_send()
+            ref = full.at[0 : (lines - 1) * size // 2, :]
+            remote(ref, ref, y_send.at[n], y_recv.at[0, 0], to_y).wait_send()
             for way in range(2):
                 for shards in range(1, lines):
 
                     @pl.when((z + 1 if way == 0 else lines - z) == shards)
                     def _():
-                        ref = some_rows(g, shards * heights[g] // 2)
-                        remote(ref, ref, z_send.at[way, g], z_recv.at[0, 0], to_z[way]).wait_send()
+                        ref = full.at[0 : shards * size // 2, :]
+                        remote(ref, ref, z_send.at[way, n], z_recv.at[0, 0], to_z[way]).wait_send()
 
         remote(tok_own, tok_other, x_send.at[0], x_recv.at[0], to_x).wait_send()
         remote(attended, att_other, att_send.at[0], att_recv.at[0], to_x).wait_send()
 
     wide = 512
-    for k in range(chunks):
-        mine = slice(k * CHUNK, (k + 1) * CHUNK)
+    for i, (begin, size) in enumerate(tails):
+        mine = slice(begin, begin + size)
         with jax.named_scope("conv_wait"):
-            conv_copy(k).wait_recv()
+            conv_copy(i).wait_recv()
 
         with jax.named_scope("last"):
             for j in range(part // wide):
@@ -762,7 +804,7 @@
     freq = jnp.asarray(np.tile(freq, LANES // half)[None, :], f32)
     chunks, blocks = rows // CHUNK, rows // WINDOW
     dma = pltpu.SemaphoreType.DMA
-    hops = (lines - 1, sum(UNITS))
+    hops = (lines - 1, sum(UNITS[:3]))
     kinds = len(UNITS)
     vmem = pl.BlockSpec(memory_space=pltpu.VMEM)
     hbm = pl.BlockSpec(memory_space=pl.ANY)
@@ -799,9 +841,9 @@
             pltpu.VMEM((rows, q_width), bf16),
             pltpu.VMEM((rows, q_width), bf16),
         ]
-        + [dma((2, kinds)), dma(hops), dma((kinds,)), dma(hops), dma((kinds,)), dma((kinds,))]
-        + [dma((1,)), dma((chunks + 1,)), dma((kinds,)), dma((chunks + 1,)), dma((6,))]
-        + [dma((3, 2)), dma((3, 2)), dma((1,)), dma((chunks,)), dma((1,)), dma((blocks,))],
+        + [dma((2, 2)), dma(hops), dma((2,)), dma(hops), dma((2,)), dma((kinds + 1,))]
+        + [dma((1,)), dma((chunks + 1,)), dma((2,)), dma((1,)), dma((2,))]
+        + [dma((3, 2)), dma((3, 2)), dma((1,)), dma((chunks + 1,)), dma((1,)), dma((1,))],
         compiler_params=pltpu.CompilerParams(
             collective_id=0, has_side_effects=True, vmem_limit_bytes=62 * 1024 * 1024
         ),

time: 76.1 us -> 75.6 us (level)
  no operation moved by 1% of the time
where the time goes in v4:
time: 75.6 us; the launch traced here: 75.4 us
  Pallas kernels  74.3 us (98%)
  local copies, waits for them, and re-layouts  1.15 us (2%)
    pallas_call x1, Pallas kernels, fused_layer(): pl.pallas_call(functools.partial(layer_kernel, (lines, rp, ro)), out_shap...  74.3 us

profile of v4, /device:TPU:0, one launch (start us, length us, event | category | flops | bytes accessed | tf_op | source)
XLA Modules:
  0.0 75.4 jit_solution(17438573147709998830)
XLA Ops:
  0.0 74.3 %layer.1 = bf16[768,1024]{1,0:T(8,128)(2,1)S(1)} custom-call(bf16[768,1024]{1,0:T(8,128)(2,1)} %tok_hbm.1, f32[1,2048]{1,0:T(1,128)} %bitcast.3, bf16[256,128]{1,0:T(8,128)(2,1)} %wk_ref.1, bf16[256,128]{1,0:T(8,128)(2,1)} %wv_ref.1, bf16[256,512]{1,0:T(8,128)(2,1)} %wc_ref.1, bf16[256,512]{1,0:T(8,128)(2,1)} %wu_ref.1, bf16[256,512]{1,0:T(8,128)(2,1)} %wb_ref.1, ...), custom_call_target="tpu_custom_call" | custom-call | flops 7247757312 | tf_op jit(solution)/shard_map/layer/pallas_call | solution.py:812
  74.3 1.1 %copy.17 = bf16[768,1024]{1,0:T(8,128)(2,1)} copy(bf16[768,1024]{1,0:T(8,128)(2,1)S(1)} %layer.1) | data formatting | bytes 3145728
